TPU v7x, 32 devices: a whole 2x2x4 slice. The times are simulated.
32 devices in a mesh: sp: 8 (over z, x), tp: 4 (over y, core).
Axes of the slice: x: 2, y: 2, z: 4, core: 2. Of those that a mesh axis runs over, the one named last changes fastest.
Arguments:
- queries: bfloat16 [4096, 512], P('sp', 'tp'), may hold values from -16 to 16
- key_heads: bfloat16 [4096, 512], P('sp', 'tp'), may hold values from -16 to 16
- value_heads: bfloat16 [4096, 512], P('sp', 'tp'), may hold values from -6 to 6
- head_gain: float32 [512], P('tp'), may hold values from 0.1 to 1.9
- residual: bfloat16 [4096, 2048], P(('sp', 'tp')), may hold values from -6 to 6
- out_weight: bfloat16 [512, 2048], replicated, may hold values from -0.25 to 0.25
- norm_gain: float32 [2048], replicated, may hold values from 0.1 to 1.9
- shared_gate: bfloat16 [2048, 512], replicated, may hold values from -0.125 to 0.125
- shared_up: bfloat16 [2048, 512], replicated, may hold values from -0.125 to 0.125
- shared_down: bfloat16 [512, 2048], replicated, may hold values from -0.25 to 0.25
- expert_gate: bfloat16 [64, 2048, 512], P(('sp', 'tp')), may hold values from -0.125 to 0.125
- expert_up: bfloat16 [64, 2048, 512], P(('sp', 'tp')), may hold values from -0.125 to 0.125
- expert_down: bfloat16 [64, 512, 2048], P(('sp', 'tp')), may hold values from -0.25 to 0.25
- routed_experts: int32 [4096, 4], P(('sp', 'tp')), may hold values from 0 to 63, all different within a row; in each aligned block of 128 rows (0 to 127, 128 to 255, ...) at most 12 rows name the same one
- route_weights: float32 [4096, 4], P(('sp', 'tp')), may hold values from 0.1 to 1.5
Outputs:
- layer_output: bfloat16 [4096, 2048], P(('sp', 'tp'))
Inputs may be any that keep to these rules, and one draw needn't show every extreme that they name: `routed_experts`: each row names 4 different experts. Within the rows of one device (128 consecutive rows, aligned) no expert is named more than 12 times, and in every draw some expert is named exactly 12 times in some device's rows.
All inputs are finite; a program needn't handle non-finite values.
Results may differ from a plain program's by a relative error of at most 0.014.
Values may be sent and summed in bfloat16 or wider, within the bound.
A program may use at most 128 MiB of HBM per device.

v0:
```python
import functools
import math

import jax
import jax.numpy as jnp
from jax import lax
from jax.experimental import pallas as pl
from jax.experimental.pallas import tpu as pltpu
from jax.sharding import PartitionSpec as P

HEAD_DIM = 64


EPSILON = 1e-06

COLUMNS = 2
TILE = 256
LOG2E = 1.4426950408889634
MESH = pl.DeviceIdType.MESH


def attention_kernel(rows, q_ref, kv_ref, gain_ref, out_ref, held, masked, acc, carry, up_send, up_recv, side_send, side_recv):
    me = lax.axis_index("sp")
    row, col = me // COLUMNS, me % COLUMNS
    seq, width = q_ref.shape
    heads = width // HEAD_DIM
    tile = min(TILE, seq)
    tiles = seq // tile
    other = row * COLUMNS + (COLUMNS - 1 - col)

    barrier = pltpu.get_barrier_semaphore()

    @pl.when(row < rows - 1)
    def _():
        pl.semaphore_signal(barrier, inc=1, device_id={"sp": me + COLUMNS}, device_id_type=MESH)

    @pl.when(row > 0)
    def _():
        pl.semaphore_signal(barrier, inc=1, device_id={"sp": me - COLUMNS}, device_id_type=MESH)

    pl.semaphore_signal(barrier, inc=1, device_id={"sp": other}, device_id_type=MESH)
    inner = (row > 0) & (row < rows - 1)

    @pl.when(inner)
    def _():
        pl.semaphore_wait(barrier, 3)

    @pl.when(jnp.logical_not(inner))
    def _():
        pl.semaphore_wait(barrier, min(rows, 2))

    def up_copy(source, depth):
        place = (row - depth) * COLUMNS + col
        return pltpu.make_async_remote_copy(
            src_ref=source, dst_ref=held.at[place], send_sem=up_send.at[depth], recv_sem=up_recv.at[depth],
            device_id={"sp": me + COLUMNS}, device_id_type=MESH)

    def side_copy(source, depth):
        place = (row - depth) * COLUMNS + col
        return pltpu.make_async_remote_copy(
            src_ref=source, dst_ref=held.at[place], send_sem=side_send.at[depth], recv_sem=side_recv.at[depth],
            device_id={"sp": other}, device_id_type=MESH)

    @pl.when(row < rows - 1)
    def _():
        up_copy(kv_ref, 0).start()

    @pl.when(col == 0)
    def _():
        side_copy(kv_ref, 0).start()

    lane = lax.broadcasted_iota(jnp.int32, (1, width), 1) // HEAD_DIM
    key_row = lax.broadcasted_iota(jnp.int32, (tile, tile), 0)
    key_col = lax.broadcasted_iota(jnp.int32, (tile, tile), 1)
    later = (key_row > key_col).astype(jnp.bfloat16)
    scale = LOG2E / math.sqrt(HEAD_DIM)

    for head in range(heads):
        for query_tile in range(tiles):
            source_rows = slice(query_tile * tile, (query_tile + 1) * tile)
            stacked_rows = slice((query_tile * heads + head) * tile, (query_tile * heads + head + 1) * tile)
            masked[stacked_rows, :] = jnp.where(lane == head, q_ref[source_rows, :], jnp.zeros((), q_ref.dtype))

    def span(source, key_tile, first, last, diagonal):
        stacked_rows = slice(first * heads * tile, last * heads * tile)
        key_rows = slice(key_tile * tile, (key_tile + 1) * tile)
        keys = source[key_rows, :width]
        values = source[key_rows, width:]
        scores = lax.dot_general(masked[stacked_rows, :], keys, (((1,), (1,)), ((), ())), preferred_element_type=jnp.float32) * scale
        soft = jnp.log2(1.0 + jnp.exp2(-jnp.abs(scores)))
        take = jnp.minimum(scores, 0.0) - soft
        stay = take - scores
        if diagonal:
            query_place = jnp.concatenate([key_row] * ((last - first) * heads), axis=0)
            key_place = jnp.concatenate([key_col] * ((last - first) * heads), axis=0)
            stay = jnp.where(key_place < query_place, stay, 0.0)
        high = stay.astype(jnp.bfloat16)
        low = (stay - high.astype(jnp.float32)).astype(jnp.bfloat16)
        after = jnp.dot(high, later, preferred_element_type=jnp.float32) + jnp.dot(low, later, preferred_element_type=jnp.float32)
        before = carry[stacked_rows, :]
        weights = jnp.exp2(take + after + before)
        if diagonal:
            weights = jnp.where(key_place < query_place, weights, 0.0)
        acc[stacked_rows, :] += jnp.dot(weights.astype(jnp.bfloat16), values, preferred_element_type=jnp.float32)
        carry[stacked_rows, :] = before + (after[:, :1] + stay[:, :1])

    acc[...] = jnp.zeros_like(acc)
    carry[...] = jnp.zeros_like(carry)
    for key_tile in range(tiles - 1, -1, -1):
        span(kv_ref, key_tile, key_tile, key_tile + 1, True)
        if key_tile + 1 < tiles:
            span(kv_ref, key_tile, key_tile + 1, tiles, False)

    def receive(depth):
        place = (row - depth) * COLUMNS + col
        up_copy(held.at[place], depth - 1).wait_recv()

        @pl.when(row < rows - 1)
        def _():
            up_copy(held.at[place], depth).start()

        side_copy(held.at[place], depth).start()

    def step(index, unused):
        shard = me - 1 - index
        depth = row - shard // COLUMNS

        @pl.when(shard % COLUMNS != col)
        def _():
            @pl.when(depth + col <= row)
            def _():
                receive(depth + col)

            side_copy(held.at[shard], depth).wait_recv()

        source = held.at[shard]
        for key_tile in range(tiles - 1, -1, -1):
            span(source, key_tile, 0, tiles, False)
        return unused

    lax.fori_loop(0, me, step, 0)

    def finish(depth, unused):
        @pl.when(row < rows - 1)
        def _():
            up_copy(kv_ref, depth).wait_send()

        @pl.when((col == 0) | (depth > 0))
        def _():
            side_copy(kv_ref, depth).wait_send()

        return unused

    lax.fori_loop(0, row + 1, finish, 0)

    for query_tile in range(tiles):
        mixed = jnp.zeros((tile, width), jnp.float32)
        inverse = jnp.zeros((tile, width), jnp.float32)
        for head in range(heads):
            place = (query_tile * heads + head) * tile
            own = jnp.where(lane == head, acc[place : place + tile, :], 0.0)
            mean = jnp.sum(own * own, axis=1, keepdims=True) * (1.0 / HEAD_DIM)
            mixed = mixed + own
            inverse = jnp.where(lane == head, lax.rsqrt(mean + EPSILON), inverse)
        out_ref[query_tile * tile : (query_tile + 1) * tile, :] = (mixed * inverse * gain_ref[...]).astype(out_ref.dtype)


def attention(queries, key_heads, value_heads, head_gain):
    seq, width = queries.shape
    shards = lax.axis_size("sp")
    rows = shards // COLUMNS
    heads = width // HEAD_DIM
    both = jnp.concatenate([key_heads, value_heads], axis=1)
    vmem = pl.BlockSpec(memory_space=pltpu.VMEM)
    return pl.pallas_call(
        functools.partial(attention_kernel, rows),
        out_shape=jax.ShapeDtypeStruct((seq, width), jnp.bfloat16),
        in_specs=[vmem] * 3,
        out_specs=vmem,
        scratch_shapes=[
            pltpu.VMEM((shards, seq, 2 * width), jnp.bfloat16),
            pltpu.VMEM((heads * seq, width), jnp.bfloat16),
            pltpu.VMEM((heads * seq, width), jnp.float32),
            pltpu.VMEM((heads * seq, 1), jnp.float32),
            pltpu.SemaphoreType.DMA((rows,)),
            pltpu.SemaphoreType.DMA((rows,)),
            pltpu.SemaphoreType.DMA((rows,)),
            pltpu.SemaphoreType.DMA((rows,)),
        ],
        compiler_params=pltpu.CompilerParams(collective_id=0, has_side_effects=True),
        name="attention",
    )(queries, both, head_gain.reshape(1, width))


def round_up(value, unit):
    return (value + unit - 1) // unit * unit


def routed_sum(expert_input, expert_gate, expert_up, expert_down, routed_experts, route_weights):
    row_count, pick_count = routed_experts.shape
    local_experts = expert_gate.shape[0]
    model_width = expert_input.shape[1]
    device_count = lax.axis_size("sp") * lax.axis_size("tp")
    expert_count = local_experts * device_count
    capacity = max(2, 3 * row_count * pick_count // (2 * expert_count))
    span = round_up(local_experts * capacity, 8)
    flat_experts = routed_experts.reshape(-1)
    expert_table = (
        flat_experts[:, None] == jnp.arange(expert_count, dtype=jnp.int32)[None, :]
    ).astype(jnp.bfloat16)
    pick_row = lax.broadcasted_iota(jnp.int32, (flat_experts.shape[0],) * 2, 0)
    pick_col = lax.broadcasted_iota(jnp.int32, (flat_experts.shape[0],) * 2, 1)
    earlier = (pick_col < pick_row).astype(jnp.bfloat16)
    counts = jnp.dot(earlier, expert_table, preferred_element_type=jnp.float32)
    ranking = jnp.sum(counts * expert_table.astype(jnp.float32), axis=1).astype(jnp.int32)
    slot_index = (flat_experts // local_experts) * span + (flat_experts % local_experts) * capacity + ranking
    match = (
        slot_index.reshape(row_count, pick_count)[:, :, None]
        == jnp.arange(device_count * span, dtype=jnp.int32)[None, None, :]
    )
    token_place = jnp.sum(match.astype(jnp.float32), axis=1).astype(jnp.bfloat16)
    outgoing = jnp.einsum(
        "rs,rd->sd", token_place, expert_input, preferred_element_type=jnp.float32
    ).astype(jnp.bfloat16)
    outgoing = outgoing.reshape(device_count, span, model_width)
    arrived = lax.all_to_all(outgoing, ("sp", "tp"), split_axis=0, concat_axis=0, tiled=True)
    places = lax.broadcasted_iota(jnp.int32, (1, span, 1), 1)
    result = jnp.zeros(arrived.shape, jnp.bfloat16)
    for expert in range(local_experts):
        first = expert * capacity // 8 * 8
        last = round_up((expert + 1) * capacity, 8)
        grouped = arrived[:, first:last].reshape(-1, model_width)
        gate_part = jnp.dot(grouped, expert_gate[expert], preferred_element_type=jnp.float32)
        up_part = jnp.dot(grouped, expert_up[expert], preferred_element_type=jnp.float32)
        hidden = (jax.nn.silu(gate_part) * up_part).astype(jnp.bfloat16)
        down = jnp.dot(hidden, expert_down[expert], preferred_element_type=jnp.float32).astype(jnp.bfloat16)
        down = jnp.pad(down.reshape(device_count, last - first, model_width), ((0, 0), (first, span - last), (0, 0)))
        mine = (places >= expert * capacity) & (places < (expert + 1) * capacity)
        result = jnp.where(mine, down, result)
    returned = lax.all_to_all(result, ("sp", "tp"), split_axis=0, concat_axis=0, tiled=True)
    returned = returned.reshape(-1, model_width)
    token_weight = jnp.sum(jnp.where(match, route_weights[:, :, None], 0.0), axis=1)
    high = token_weight.astype(jnp.bfloat16)
    low = (token_weight - high.astype(jnp.float32)).astype(jnp.bfloat16)
    both = jnp.dot(jnp.concatenate([high, low], axis=0), returned, preferred_element_type=jnp.float32)
    return both[:row_count] + both[row_count:]


def body(
    queries,
    key_heads,
    value_heads,
    head_gain,
    residual,
    out_weight,
    norm_gain,
    shared_gate,
    shared_up,
    shared_down,
    expert_gate,
    expert_up,
    expert_down,
    routed_experts,
    route_weights,
):
    head_output = attention(queries, key_heads, value_heads, head_gain)
    token_heads = lax.all_to_all(head_output, "tp", split_axis=0, concat_axis=1, tiled=True)
    branch = jnp.dot(token_heads, out_weight, preferred_element_type=jnp.float32)
    stream = (residual.astype(jnp.float32) + branch).astype(jnp.bfloat16)
    stream_wide = stream.astype(jnp.float32)
    inverse = lax.rsqrt(jnp.mean(stream_wide * stream_wide, axis=1, keepdims=True) + EPSILON)
    expert_input = (stream_wide * inverse * norm_gain).astype(jnp.bfloat16)
    shared_hidden = (
        jax.nn.silu(jnp.dot(expert_input, shared_gate, preferred_element_type=jnp.float32))
        * jnp.dot(expert_input, shared_up, preferred_element_type=jnp.float32)
    ).astype(jnp.bfloat16)
    shared_term = jnp.dot(shared_hidden, shared_down, preferred_element_type=jnp.float32)
    routed = routed_sum(
        expert_input, expert_gate, expert_up, expert_down, routed_experts, route_weights
    )
    return (stream_wide + shared_term + routed).astype(jnp.bfloat16)


def solution(mesh):
    return jax.shard_map(
        body,
        mesh=mesh,
        in_specs=(
            P("sp", "tp"),
            P("sp", "tp"),
            P("sp", "tp"),
            P("tp"),
            P(("sp", "tp"), None),
            P(),
            P(),
            P(),
            P(),
            P(),
            P(("sp", "tp"), None, None),
            P(("sp", "tp"), None, None),
            P(("sp", "tp"), None, None),
            P(("sp", "tp"), None),
            P(("sp", "tp"), None),
        ),
        out_specs=P(("sp", "tp"), None),
        check_vma=False,
    )
```

profile of v0, /device:TPU:0, one launch (start us, length us, event | category | flops | bytes accessed | tf_op | source)
XLA Modules:
  0.0 241.9 jit_solution(2011154182114934235)
XLA Ops:
  0.0 0.0 copy-start
  0.0 0.0 copy-start.6
  0.0 0.0 copy-start.7
  0.0 1.8 pad_maximum_fusion.kv_ref
  1.9 10.7 %attention.1 = bf16[512,128]{1,0:T(8,128)(2,1)} custom-call(bf16[512,128]{1,0:T(8,128)(2,1)} %q_ref.1, bf16[512,256]{1,0:T(8,128)(2,1)} %pad_maximum_fusion.kv_ref, f32[1,128]{1,0:T(1,128)} %bitcast.61), custom_call_target="tpu_custom_call" | custom-call | tf_op jit(solution)/shard_map/attention/pallas_call | solution.py:175
  12.5 1.7 copy.38
  14.2 3.3 %all-to-all-start = ((bf16[4,128,128]{1,2,0:T(8,128)(2,1)}), bf16[4,128,128]{1,2,0:T(8,128)(2,1)S(1)}, u32[]{:S(2)}, u32[]{:S(2)}) async-start(bf16[4,128,128]{1,2,0:T(8,128)(2,1)} %copy.38), calls=%async_computation | async-start | bytes 262144 | tf_op jit(solution)/shard_map/all_to_all | solution.py:267
  17.5 0.8 copy.39
  18.3 0.1 eq.30
  18.4 0.3 fusion.33
  18.7 0.1 convert_element_type.75
  18.8 0.1 copy.40
  18.9 0.0 copy-done.6
  18.9 0.0 copy-done.7
  18.9 0.0 copy-start.5
  18.9 1.0 select_reduce_fusion
  20.0 2.1 all-to-all-done
  22.1 0.0 copy-start.4
  22.1 0.6 copy-done.4
  22.7 0.0 copy-start.3
  22.7 0.0 copy-done
  22.7 1.7 multiply_reduce_fusion
  24.4 0.0 copy-done.5
  24.5 0.0 copy-done.3
  24.5 2.8 %convolution_convert_fusion = bf16[768,2048]{1,0:T(8,128)(2,1)} fusion(bf16[128,768]{1,0:T(8,128)(2,1)S(1)} %copy-done.3, f32[128,2048]{1,0:T(8,128)S(1)} %get-tuple-element.12, f32[2048]{0:T(1024)S(1)} %copy-done.5, f32[128]{0:T(128)S(1)} %add_rsqrt_fusion), kind=kOutput, calls=%fused_computation | convolution fusion | flops 405012480 | bytes 4399616 | tf_op jit(solution)/shard_map/rs,rd->sd/dot_general | solution.py:222
  27.2 30.9 %all-to-all-start.1 = ((bf16[32,24,2048]{2,1,0:T(8,128)(2,1)}), bf16[32,24,2048]{2,1,0:T(8,128)(2,1)}, u32[]{:S(2)}, u32[]{:S(2)}) async-start(bf16[32,24,2048]{2,1,0:T(8,128)(2,1)} %bitcast.52), calls=%async_computation.1 | async-start | bytes 6291456 | tf_op jit(solution)/shard_map/all_to_all | solution.py:226
  58.2 0.5 compare_and_fusion
  58.7 70.9 %all-to-all-done.1 = bf16[32,24,2048]{2,1,0:T(8,128)(2,1)} async-done(((bf16[32,24,2048]{2,1,0:T(8,128)(2,1)}), bf16[32,24,2048]{2,1,0:T(8,128)(2,1)}, u32[]{:S(2)}, u32[]{:S(2)}) %all-to-all-start.1) | async-done | bytes 3145760 | tf_op jit(solution)/shard_map/all_to_all | solution.py:226
  129.6 0.0 copy-start.8
  129.6 2.9 %fusion.64 = (bf16[32,16,2048]{2,1,0:T(8,128)(2,1)S(1)}, bf16[32,16,2048]{2,1,0:T(8,128)(2,1)S(1)}) fusion(bf16[32,24,2048]{2,1,0:T(8,128)(2,1)} %all-to-all-done.1), kind=kLoop, calls=%fused_computation.79 | loop fusion | bytes 8388608 | tf_op jit(solution)/shard_map/slice | solution.py:232
  132.5 0.0 copy-start.2
  132.5 0.0 copy-start.1
  132.5 0.5 copy-done.8
  133.0 2.3 fusion.12
  135.3 0.0 copy-done.2
  135.3 0.0 copy-done.1
  135.3 2.2 fusion.7
  137.5 7.0 %convolution_convert_fusion.2 = bf16[512,2048]{1,0:T(8,128)(2,1)} fusion(bf16[2,512,2048]{2,1,0:T(8,128)(2,1)} %param.27, bf16[512,2048]{1,0:T(8,128)(2,1)} %bitcast.58, bf16[2,2048,512]{2,1,0:T(8,128)(2,1)} %param.26, f32[512,512]{1,0:T(8,128)} %fusion.12), kind=kOutput, calls=%fused_computation.3 | convolution fusion | flops 2150105088 | bytes 9437184 | tf_op jit(solution)/shard_map/dot_general | solution.py:236
  144.5 7.0 %convolution_convert_fusion.1 = bf16[512,2048]{1,0:T(8,128)(2,1)} fusion(bf16[2,512,2048]{2,1,0:T(8,128)(2,1)} %param.27, bf16[512,2048]{1,0:T(8,128)(2,1)} %bitcast.55, bf16[2,2048,512]{2,1,0:T(8,128)(2,1)} %param.26, f32[512,512]{1,0:T(8,128)} %fusion.7), kind=kOutput, calls=%fused_computation.2 | convolution fusion | flops 2150105088 | bytes 9437184 | tf_op jit(solution)/shard_map/dot_general | solution.py:236
  151.4 5.2 %select_select_fusion = bf16[32,24,2048]{2,1,0:T(8,128)(2,1)} fusion(bf16[32,16,2048]{2,1,0:T(8,128)(2,1)} %bitcast.56, bf16[32,16,2048]{2,1,0:T(8,128)(2,1)} %bitcast.53, pred[24]{0:T(512)(128)(4,1)} %get-tuple-element.14, pred[24]{0:T(512)(128)(4,1)S(1)} %get-tuple-element.13), kind=kLoop, calls=%fused_computation.1 | loop fusion | flops 3145728 | bytes 7340080 | tf_op jit(solution)/shard_map/jit(_where)/select_n | solution.py:239
  156.6 4.7 %all-to-all-start.2 = ((bf16[32,24,2048]{2,1,0:T(8,128)(2,1)}), bf16[32,24,2048]{2,1,0:T(8,128)(2,1)}, u32[]{:S(2)}, u32[]{:S(2)}) async-start(bf16[32,24,2048]{2,1,0:T(8,128)(2,1)} %select_select_fusion), calls=%async_computation.2 | async-start | bytes 6291456 | tf_op jit(solution)/shard_map/all_to_all | solution.py:240
  161.3 0.8 subtract_convert_fusion
  162.1 2.1 fusion.63
  164.2 68.7 %all-to-all-done.2 = bf16[32,24,2048]{2,1,0:T(8,128)(2,1)} async-done(((bf16[32,24,2048]{2,1,0:T(8,128)(2,1)}), bf16[32,24,2048]{2,1,0:T(8,128)(2,1)}, u32[]{:S(2)}, u32[]{:S(2)}) %all-to-all-start.2) | async-done | bytes 3145760 | tf_op jit(solution)/shard_map/all_to_all | solution.py:240
  232.9 4.4 %fusion.40 = f32[256,2048]{1,0:T(8,128)} fusion(bf16[768,2048]{1,0:T(8,128)(2,1)} %bitcast.15, bf16[128,768]{1,0:T(8,128)(2,1)} %get-tuple-element.7, bf16[128,768]{1,0:T(8,128)(2,1)} %get-tuple-element.8), kind=kOutput, calls=%fused_computation.43 | convolution fusion | flops 806092800 | bytes 5636096 | tf_op jit(solution)/shard_map/dot_general | solution.py:245
  237.3 4.5 %fusion.3 = bf16[128,2048]{1,0:T(8,128)(2,1)} fusion(f32[128,2048]{1,0:T(8,128)S(1)} %get-tuple-element.12, bf16[512,2048]{1,0:T(8,128)(2,1)} %param.24, bf16[2048,512]{1,0:T(8,128)(2,1)} %param.23, f32[256,2048]{1,0:T(8,128)} %fusion.40, f32[128,512]{1,0:T(8,128)S(1)} %fusion.63, f32[2048]{0:T(1024)S(1)} %copy-done.5, f32[128]{0:T(128)S(1)} %add_rsqrt_fusion), kind=kOutput, calls=%fused_computation.9 | convolution fusion | flops 539099136 | bytes 9183744 | tf_op jit(solution)/shard_map/dot_general | solution.py:277
  (3 shorter events, 0.0 us)
Async XLA Ops:
  0.0 22.7 %copy-start = (bf16[512,2048]{1,0:T(8,128)(2,1)S(1)}, bf16[512,2048]{1,0:T(8,128)(2,1)}, u32[]{:S(2)}) copy-start(bf16[512,2048]{1,0:T(8,128)(2,1)} %param.20) | copy-start | bytes 6291460
  0.0 18.9 %copy-start.6 = (s32[128,4]{0,1:T(4,128)S(1)}, s32[128,4]{0,1:T(4,128)}, u32[]{:S(2)}) copy-start(s32[128,4]{0,1:T(4,128)} %param.28) | copy-start | bytes 6148
  0.0 18.9 %copy-start.7 = (f32[128,4]{0,1:T(4,128)S(1)}, f32[128,4]{0,1:T(4,128)}, u32[]{:S(2)}) copy-start(f32[128,4]{0,1:T(4,128)} %param.29) | copy-start | bytes 6148
  14.2 7.9 %all-to-all-start = ((bf16[4,128,128]{1,2,0:T(8,128)(2,1)}), bf16[4,128,128]{1,2,0:T(8,128)(2,1)S(1)}, u32[]{:S(2)}, u32[]{:S(2)}) async-start(bf16[4,128,128]{1,2,0:T(8,128)(2,1)} %copy.38), calls=%async_computation | async-start | bytes 262144 | tf_op jit(solution)/shard_map/all_to_all | solution.py:267
  18.9 5.5 %copy-start.5 = (f32[2048]{0:T(1024)S(1)}, f32[2048]{0:T(1024)}, u32[]{:S(2)}) copy-start(f32[2048]{0:T(1024)} %param.21) | copy-start | bytes 24580
  22.1 0.7 copy-start.4
  22.7 1.7 copy-start.3
  27.2 102.4 %all-to-all-start.1 = ((bf16[32,24,2048]{2,1,0:T(8,128)(2,1)}), bf16[32,24,2048]{2,1,0:T(8,128)(2,1)}, u32[]{:S(2)}, u32[]{:S(2)}) async-start(bf16[32,24,2048]{2,1,0:T(8,128)(2,1)} %bitcast.52), calls=%async_computation.1 | async-start | bytes 6291456 | tf_op jit(solution)/shard_map/all_to_all | solution.py:226
  129.6 3.5 %copy-start.8 = (bf16[2,2048,512]{2,1,0:T(8,128)(2,1)S(1)}, bf16[2,2048,512]{2,1,0:T(8,128)(2,1)}, u32[]{:S(2)}) copy-start(bf16[2,2048,512]{2,1,0:T(8,128)(2,1)} %param.25) | copy-start | bytes 12582916
  132.5 2.8 %copy-start.2 = (bf16[32,16,2048]{2,1,0:T(8,128)(2,1)}, bf16[32,16,2048]{2,1,0:T(8,128)(2,1)S(1)}, u32[]{:S(2)}) copy-start(bf16[32,16,2048]{2,1,0:T(8,128)(2,1)S(1)} %get-tuple-element.9) | copy-start | bytes 6291460
  132.5 2.8 %copy-start.1 = (bf16[32,16,2048]{2,1,0:T(8,128)(2,1)}, bf16[32,16,2048]{2,1,0:T(8,128)(2,1)S(1)}, u32[]{:S(2)}) copy-start(bf16[32,16,2048]{2,1,0:T(8,128)(2,1)S(1)} %get-tuple-element.10) | copy-start | bytes 6291460
  156.6 76.3 %all-to-all-start.2 = ((bf16[32,24,2048]{2,1,0:T(8,128)(2,1)}), bf16[32,24,2048]{2,1,0:T(8,128)(2,1)}, u32[]{:S(2)}, u32[]{:S(2)}) async-start(bf16[32,24,2048]{2,1,0:T(8,128)(2,1)} %select_select_fusion), calls=%async_computation.2 | async-start | bytes 6291456 | tf_op jit(solution)/shard_map/all_to_all | solution.py:240
where the time goes:
time: 242 us
  waiting for transfers between devices  142 us (59%)
  starting transfers between devices  39 us (16%)
  matrix products  34.2 us (14%)
  Pallas kernels  10.7 us (4%)
  other arithmetic  9.39 us (4%)
  local copies, waits for them, and re-layouts  6.83 us (3%)
    all_to_all x1, waiting for transfers between devices, routed_sum(): lax.all_to_all(outgoing, ('sp', 'tp'), split_axis=0, concat_axis=0, tiled...  70.9 us
    all_to_all x1, waiting for transfers between devices, routed_sum(): lax.all_to_all(result, ('sp', 'tp'), split_axis=0, concat_axis=0, tiled=T...  68.7 us
    all_to_all x1, starting transfers between devices, routed_sum(): lax.all_to_all(outgoing, ('sp', 'tp'), split_axis=0, concat_axis=0, tiled...  30.9 us
    dot_general x2, matrix products, routed_sum(): jnp.dot(hidden, expert_down[expert], preferred_element_type=jnp.float32)  13.9 us
    pallas_call x1, Pallas kernels, attention(): pl.pallas_call(functools.partial(attention_kernel, rows), out_shape=jax.S...  10.7 us
    select_n x1, other arithmetic, routed_sum(): result = jnp.where(mine, down, result)  5.17 us
  transfers between devices with their start and end apart: 3, of which 3 were waited for; matrix products, arithmetic and copies ran while one was open for 2% of the time, Pallas kernels for 0%

commit v1 on v0

--- a/solution.py
+++ b/solution.py
@@ -17,6 +17,9 @@
 TILE = 256
 LOG2E = 1.4426950408889634
 MESH = pl.DeviceIdType.MESH
+CHUNKS = 8
+LAG = 2
+VMEM_LIMIT = 67043328
 
 
 def attention_kernel(rows, q_ref, kv_ref, gain_ref, out_ref, held, masked, acc, carry, up_send, up_recv, side_send, side_recv):
@@ -196,54 +199,356 @@
     return (value + unit - 1) // unit * unit
 
 
-def routed_sum(expert_input, expert_gate, expert_up, expert_down, routed_experts, route_weights):
-    row_count, pick_count = routed_experts.shape
-    local_experts = expert_gate.shape[0]
-    model_width = expert_input.shape[1]
-    device_count = lax.axis_size("sp") * lax.axis_size("tp")
-    expert_count = local_experts * device_count
-    capacity = max(2, 3 * row_count * pick_count // (2 * expert_count))
-    span = round_up(local_experts * capacity, 8)
-    flat_experts = routed_experts.reshape(-1)
-    expert_table = (
-        flat_experts[:, None] == jnp.arange(expert_count, dtype=jnp.int32)[None, :]
-    ).astype(jnp.bfloat16)
-    pick_row = lax.broadcasted_iota(jnp.int32, (flat_experts.shape[0],) * 2, 0)
-    pick_col = lax.broadcasted_iota(jnp.int32, (flat_experts.shape[0],) * 2, 1)
-    earlier = (pick_col < pick_row).astype(jnp.bfloat16)
-    counts = jnp.dot(earlier, expert_table, preferred_element_type=jnp.float32)
-    ranking = jnp.sum(counts * expert_table.astype(jnp.float32), axis=1).astype(jnp.int32)
-    slot_index = (flat_experts // local_experts) * span + (flat_experts % local_experts) * capacity + ranking
-    match = (
-        slot_index.reshape(row_count, pick_count)[:, :, None]
-        == jnp.arange(device_count * span, dtype=jnp.int32)[None, None, :]
-    )
-    token_place = jnp.sum(match.astype(jnp.float32), axis=1).astype(jnp.bfloat16)
-    outgoing = jnp.einsum(
-        "rs,rd->sd", token_place, expert_input, preferred_element_type=jnp.float32
-    ).astype(jnp.bfloat16)
-    outgoing = outgoing.reshape(device_count, span, model_width)
-    arrived = lax.all_to_all(outgoing, ("sp", "tp"), split_axis=0, concat_axis=0, tiled=True)
-    places = lax.broadcasted_iota(jnp.int32, (1, span, 1), 1)
-    result = jnp.zeros(arrived.shape, jnp.bfloat16)
-    for expert in range(local_experts):
-        first = expert * capacity // 8 * 8
-        last = round_up((expert + 1) * capacity, 8)
-        grouped = arrived[:, first:last].reshape(-1, model_width)
-        gate_part = jnp.dot(grouped, expert_gate[expert], preferred_element_type=jnp.float32)
-        up_part = jnp.dot(grouped, expert_up[expert], preferred_element_type=jnp.float32)
-        hidden = (jax.nn.silu(gate_part) * up_part).astype(jnp.bfloat16)
-        down = jnp.dot(hidden, expert_down[expert], preferred_element_type=jnp.float32).astype(jnp.bfloat16)
-        down = jnp.pad(down.reshape(device_count, last - first, model_width), ((0, 0), (first, span - last), (0, 0)))
-        mine = (places >= expert * capacity) & (places < (expert + 1) * capacity)
-        result = jnp.where(mine, down, result)
-    returned = lax.all_to_all(result, ("sp", "tp"), split_axis=0, concat_axis=0, tiled=True)
-    returned = returned.reshape(-1, model_width)
-    token_weight = jnp.sum(jnp.where(match, route_weights[:, :, None], 0.0), axis=1)
-    high = token_weight.astype(jnp.bfloat16)
-    low = (token_weight - high.astype(jnp.float32)).astype(jnp.bfloat16)
-    both = jnp.dot(jnp.concatenate([high, low], axis=0), returned, preferred_element_type=jnp.float32)
-    return both[:row_count] + both[row_count:]
+def moe_kernel(
+    rows, capacity, span, heads_ref, meta_ref, residual_ref, gain_ref, out_weight, shared_gate, shared_up, shared_down, expert_gate,
+    expert_up, expert_down, out_ref, head_rows, meta_all, slots, place, mix, inputs, gathered, outgoing, arrived, returned, landed, base,
+    gate_sum, up_sum, hidden, w_out, w_sgate, w_sup, w_sdown, w_gate, w_up, w_down, w_sem, head_send, head_recv, meta_send, meta_recv,
+    up_send, up_recv, down_send, down_recv, go_send, go_recv, back_send, back_recv, part_send, part_recv):
+    me = lax.axis_index("sp")
+    tp = lax.axis_index("tp")
+    row, col = me // COLUMNS, me % COLUMNS
+    tp_size = head_rows.shape[0]
+    group = COLUMNS * tp_size
+    mine = col * tp_size + tp
+    chunks, _, local, _, width = outgoing.shape
+    count = residual_ref.shape[0]
+    picks = meta_ref.shape[0] // 2
+    total = group * local * span
+
+    loads = []
+    for index, (source, target) in enumerate((
+            (out_weight, w_out), (expert_gate, w_gate), (expert_up, w_up), (expert_down, w_down),
+            (shared_gate, w_sgate), (shared_up, w_sup), (shared_down, w_sdown))):
+        loads.append(pltpu.make_async_copy(source, target, w_sem.at[index]))
+        loads[-1].start()
+
+    peers = []
+    for across in range(COLUMNS - 1, -1, -1):
+        for step in list(range(tp_size // 2, tp_size)) + list(range(tp_size // 2)):
+            if across or step:
+                peers.append(((col + across) % COLUMNS, (tp + step) % tp_size))
+
+    def device(at_row, at_col, at_tp):
+        return {"sp": at_row * COLUMNS + at_col, "tp": at_tp}
+
+    barrier = pltpu.get_barrier_semaphore()
+    for at_col, at_tp in peers:
+        pl.semaphore_signal(barrier, inc=1, device_id=device(row, at_col, at_tp), device_id_type=MESH)
+    for step in range(1, rows):
+        pl.semaphore_signal(barrier, inc=1, device_id=device((row + step) % rows, col, tp), device_id_type=MESH)
+    pl.semaphore_wait(barrier, len(peers) + rows - 1)
+
+    def head_copy(to, source):
+        return pltpu.make_async_remote_copy(
+            src_ref=heads_ref.at[pl.ds(pl.multiple_of(to * count, count), count), :],
+            dst_ref=head_rows.at[source], send_sem=head_send.at[to], recv_sem=head_recv.at[source],
+            device_id=device(row, col, to), device_id_type=MESH)
+
+    def meta_copy(to, source):
+        return pltpu.make_async_remote_copy(
+            src_ref=meta_ref, dst_ref=meta_all.at[source], send_sem=meta_send.at[to], recv_sem=meta_recv.at[source],
+            device_id=device(to, col, tp), device_id_type=MESH)
+
+    for step in range(1, tp_size):
+        head_copy((tp + step) % tp_size, tp).start()
+    for step in range(1, rows):
+        meta_copy((row + step) % rows, row).start()
+    head_rows[tp] = heads_ref[pl.ds(pl.multiple_of(tp * count, count), count), :]
+    meta_all[row] = meta_ref[...]
+    for step in range(1, rows):
+        meta_copy((row + step) % rows, (row + step) % rows).wait_recv()
+
+    expert_place = lax.broadcasted_iota(jnp.int32, (group * local, count), 0).astype(jnp.float32)
+    slot_place = lax.broadcasted_iota(jnp.int32, (total, count), 0).astype(jnp.float32)
+    first = lax.broadcasted_iota(jnp.int32, (count, count), 0)
+    second = lax.broadcasted_iota(jnp.int32, (count, count), 1)
+    earlier = (first < second).astype(jnp.bfloat16)
+    lowest = (row * (group * local)).astype(jnp.float32)
+    for block in range(rows):
+        meta = meta_all[block]
+        chosen = [meta[k : k + 1, :] - lowest for k in range(picks)]
+        tables = [jnp.where(expert_place == chosen[k], 1.0, 0.0) for k in range(picks)]
+        tally = jnp.dot(sum(tables).astype(jnp.bfloat16), earlier, preferred_element_type=jnp.float32)
+        placed = jnp.zeros((total, count), jnp.float32)
+        for k in range(picks):
+            ranking = jnp.sum(tables[k] * tally, axis=0, keepdims=True)
+            inside = (chosen[k] >= 0.0) & (chosen[k] < float(group * local))
+            slot = jnp.where(inside, chosen[k] * float(span) + (block * capacity + ranking), -1.0)
+            slots[block, k : k + 1, :] = slot
+            placed = jnp.where(slot_place == slot, 1.0, placed)
+        place[:, block * count : (block + 1) * count] = placed.astype(jnp.bfloat16)
+
+    loads[0].wait()
+    for step in range(1, tp_size):
+        head_copy((tp + step) % tp_size, (tp + step) % tp_size).wait_recv()
+    token_heads = jnp.concatenate([head_rows[source] for source in range(tp_size)], axis=1)
+    branch = jnp.dot(token_heads, w_out[...], preferred_element_type=jnp.float32)
+    stream = (residual_ref[...].astype(jnp.float32) + branch).astype(jnp.bfloat16).astype(jnp.float32)
+    inverse = lax.rsqrt(jnp.mean(stream * stream, axis=1, keepdims=True) + EPSILON)
+    normed = (stream * inverse * gain_ref[...]).astype(jnp.bfloat16)
+    inputs[...] = normed
+    for chunk in range(chunks):
+        columns = slice(chunk * width, (chunk + 1) * width)
+        base[chunk] = stream[:, columns]
+        gathered[chunk, row] = normed[:, columns]
+
+    def up_copy(chunk, block):
+        return pltpu.make_async_remote_copy(
+            src_ref=gathered.at[chunk, block], dst_ref=gathered.at[chunk, block], send_sem=up_send.at[chunk, block],
+            recv_sem=up_recv.at[chunk, block], device_id=device(row + 1, col, tp), device_id_type=MESH)
+
+    def down_copy(chunk, block):
+        return pltpu.make_async_remote_copy(
+            src_ref=gathered.at[chunk, block], dst_ref=gathered.at[chunk, block], send_sem=down_send.at[chunk, block],
+            recv_sem=down_recv.at[chunk, block], device_id=device(row - 1, col, tp), device_id_type=MESH)
+
+    def send_own(chunk):
+        @pl.when(row < rows - 1)
+        def _():
+            up_copy(chunk, row).start()
+
+        @pl.when(row > 0)
+        def _():
+            down_copy(chunk, row).start()
+
+    def gather(chunk):
+        for depth in range(1, rows):
+            @pl.when(row >= depth)
+            def _():
+                up_copy(chunk, row - depth).wait_recv()
+
+                @pl.when(row < rows - 1)
+                def _():
+                    up_copy(chunk, row - depth).start()
+
+            @pl.when(row + depth < rows)
+            def _():
+                down_copy(chunk, row + depth).wait_recv()
+
+                @pl.when(row > 0)
+                def _():
+                    down_copy(chunk, row + depth).start()
+
+    def go_copy(chunk, peer, source):
+        at_col, at_tp = peer
+        return pltpu.make_async_remote_copy(
+            src_ref=outgoing.at[chunk, at_col * tp_size + at_tp], dst_ref=arrived.at[chunk, :, source],
+            send_sem=go_send.at[chunk, at_col * tp_size + at_tp], recv_sem=go_recv.at[chunk, source],
+            device_id=device(row, at_col, at_tp), device_id_type=MESH)
+
+    def back_copy(chunk, peer, source):
+        at_col, at_tp = peer
+        return pltpu.make_async_remote_copy(
+            src_ref=outgoing.at[chunk, at_col * tp_size + at_tp], dst_ref=returned.at[chunk, source],
+            send_sem=back_send.at[chunk, at_col * tp_size + at_tp], recv_sem=back_recv.at[chunk, source],
+            device_id=device(row, at_col, at_tp), device_id_type=MESH)
+
+    def part_copy(chunk, block, source):
+        return pltpu.make_async_remote_copy(
+            src_ref=gathered.at[chunk, block], dst_ref=landed.at[chunk, source], send_sem=part_send.at[chunk, block],
+            recv_sem=part_recv.at[chunk, source], device_id=device(block, col, tp), device_id_type=MESH)
+
+    def dispatch(chunk):
+        tokens = gathered[chunk].reshape(rows * count, width)
+        rows_out = jnp.dot(place[...], tokens, preferred_element_type=jnp.float32).astype(jnp.bfloat16)
+        outgoing[chunk] = rows_out.reshape(group, local, span, width)
+        arrived[chunk, :, mine] = outgoing[chunk, mine]
+        for peer in peers:
+            go_copy(chunk, peer, mine).start()
+
+    def enter(chunk):
+        for peer in peers:
+            go_copy(chunk, peer, peer[0] * tp_size + peer[1]).wait_recv()
+        deep = pl.ds(pl.multiple_of(chunk * width, width), width)
+        for expert in range(local):
+            block = arrived[chunk, expert].reshape(group * span, width)
+            gate_sum[expert] += jnp.dot(block, w_gate[expert, deep, :], preferred_element_type=jnp.float32)
+            up_sum[expert] += jnp.dot(block, w_up[expert, deep, :], preferred_element_type=jnp.float32)
+
+    for chunk in range(min(2, chunks)):
+        send_own(chunk)
+    gate_sum[...] = jnp.zeros_like(gate_sum)
+    up_sum[...] = jnp.zeros_like(up_sum)
+    loads[1].wait()
+    loads[2].wait()
+
+    def forward(index, unused):
+        @pl.when(index < chunks)
+        def _():
+            gather(index)
+
+            @pl.when(index + 2 < chunks)
+            def _():
+                send_own(index + 2)
+
+            dispatch(index)
+
+        @pl.when(index >= LAG)
+        def _():
+            enter(index - LAG)
+
+        return unused
+
+    lax.fori_loop(0, chunks + LAG, forward, 0)
+
+    for expert in range(local):
+        gate = gate_sum[expert]
+        hidden[expert] = (gate / (1.0 + jnp.exp(-gate)) * up_sum[expert]).astype(jnp.bfloat16)
+
+    def sent(chunk, unused):
+        for peer in peers:
+            go_copy(chunk, peer, mine).wait_send()
+        return unused
+
+    lax.fori_loop(0, chunks, sent, 0)
+    loads[3].wait()
+
+    def leave(chunk, unused):
+        wide = pl.ds(pl.multiple_of(chunk * width, width), width)
+        for expert in range(local):
+            down = jnp.dot(hidden[expert], w_down[expert, :, wide], preferred_element_type=jnp.float32).astype(jnp.bfloat16)
+            outgoing[chunk, :, expert] = down.reshape(group, span, width)
+        returned[chunk, mine] = outgoing[chunk, mine]
+        for peer in peers:
+            back_copy(chunk, peer, mine).start()
+        return unused
+
+    lax.fori_loop(0, chunks, leave, 0)
+
+    for block in range(rows):
+        weighed = jnp.zeros((total, count), jnp.float32)
+        for k in range(picks):
+            slot = slots[block, k : k + 1, :]
+            weighed = jnp.where(slot_place == slot, meta_all[block, picks + k : picks + k + 1, :], weighed)
+        mix[block] = weighed.T.astype(jnp.bfloat16)
+
+    for load in loads[4:]:
+        load.wait()
+
+    def gathered_sent(chunk, unused):
+        @pl.when(row < rows - 1)
+        def _():
+            def one(block, inner):
+                up_copy(chunk, block).wait_send()
+                return inner
+
+            lax.fori_loop(0, row + 1, one, 0)
+
+        @pl.when(row > 0)
+        def _():
+            def one(block, inner):
+                down_copy(chunk, block).wait_send()
+                return inner
+
+            lax.fori_loop(row, rows, one, 0)
+
+        return unused
+
+    lax.fori_loop(0, chunks, gathered_sent, 0)
+    x = inputs[...]
+    shared = jnp.dot(x, w_sgate[...], preferred_element_type=jnp.float32)
+    shared = (shared / (1.0 + jnp.exp(-shared)) * jnp.dot(x, w_sup[...], preferred_element_type=jnp.float32)).astype(jnp.bfloat16)
+    for chunk in range(chunks):
+        columns = slice(chunk * width, (chunk + 1) * width)
+        base[chunk] += jnp.dot(shared, w_sdown[:, columns], preferred_element_type=jnp.float32)
+
+    def combine(chunk, unused):
+        for peer in peers:
+            back_copy(chunk, peer, peer[0] * tp_size + peer[1]).wait_recv()
+        results = returned[chunk].reshape(total, width)
+        for step in range(1, rows):
+            block = (row + step) % rows
+            gathered[chunk, block] = jnp.dot(mix[block], results, preferred_element_type=jnp.float32).astype(jnp.bfloat16)
+        base[chunk] += jnp.dot(mix[row], results, preferred_element_type=jnp.float32)
+        for step in range(1, rows):
+            part_copy(chunk, (row + step) % rows, row).start()
+        return unused
+
+    lax.fori_loop(0, chunks, combine, 0)
+
+    def close(chunk, unused):
+        value = base[chunk]
+        for step in range(1, rows):
+            source = (row + step) % rows
+            part_copy(chunk, source, source).wait_recv()
+            value += landed[chunk, source].astype(jnp.float32)
+        out_ref[:, pl.ds(pl.multiple_of(chunk * width, width), width)] = value.astype(out_ref.dtype)
+        for peer in peers:
+            back_copy(chunk, peer, mine).wait_send()
+        for step in range(1, rows):
+            part_copy(chunk, (row + step) % rows, row).wait_send()
+        return unused
+
+    lax.fori_loop(0, chunks, close, 0)
+    for step in range(1, tp_size):
+        head_copy((tp + step) % tp_size, tp).wait_send()
+    for step in range(1, rows):
+        meta_copy((row + step) % rows, row).wait_send()
+
+
+def experts(
+    head_output, residual, out_weight, norm_gain, shared_gate, shared_up, shared_down, expert_gate, expert_up, expert_down,
+    routed_experts, route_weights):
+    count, picks = routed_experts.shape
+    model = residual.shape[1]
+    sp_size, tp_size = lax.axis_size("sp"), lax.axis_size("tp")
+    rows, group = sp_size // COLUMNS, COLUMNS * tp_size
+    local, _, inner = expert_gate.shape
+    shared_inner = shared_gate.shape[1]
+    expert_count = local * sp_size * tp_size
+    capacity = max(2, 3 * count * picks // (2 * expert_count))
+    span = round_up(rows * capacity, 16)
+    total = group * local * span
+    width = model // CHUNKS
+    meta = jnp.concatenate([routed_experts.astype(jnp.float32).T, route_weights.T], axis=0)
+    vmem = pl.BlockSpec(memory_space=pltpu.VMEM)
+    hbm = pl.BlockSpec(memory_space=pl.ANY)
+    half = jnp.bfloat16
+
+    def pair(*shape):
+        return [pltpu.SemaphoreType.DMA(shape)] * 2
+
+    return pl.pallas_call(
+        functools.partial(moe_kernel, rows, capacity, span),
+        out_shape=jax.ShapeDtypeStruct((count, model), half),
+        in_specs=[vmem] * 4 + [hbm] * 7,
+        out_specs=vmem,
+        scratch_shapes=[
+            pltpu.VMEM((tp_size, count, head_output.shape[1]), half),
+            pltpu.VMEM((rows, 2 * picks, count), jnp.float32),
+            pltpu.VMEM((rows, 2 * picks, count), jnp.float32),
+            pltpu.VMEM((total, rows * count), half),
+            pltpu.VMEM((rows, count, total), half),
+            pltpu.VMEM((count, model), half),
+            pltpu.VMEM((CHUNKS, rows, count, width), half),
+            pltpu.VMEM((CHUNKS, group, local, span, width), half),
+            pltpu.VMEM((CHUNKS, local, group, span, width), half),
+            pltpu.VMEM((CHUNKS, group, local, span, width), half),
+            pltpu.VMEM((CHUNKS, rows, count, width), half),
+            pltpu.VMEM((CHUNKS, count, width), jnp.float32),
+            pltpu.VMEM((local, group * span, inner), jnp.float32),
+            pltpu.VMEM((local, group * span, inner), jnp.float32),
+            pltpu.VMEM((local, group * span, inner), half),
+            pltpu.VMEM(out_weight.shape, half),
+            pltpu.VMEM(shared_gate.shape, half),
+            pltpu.VMEM(shared_up.shape, half),
+            pltpu.VMEM(shared_down.shape, half),
+            pltpu.VMEM(expert_gate.shape, half),
+            pltpu.VMEM(expert_up.shape, half),
+            pltpu.VMEM(expert_down.shape, half),
+            pltpu.SemaphoreType.DMA((7,)),
+            *pair(tp_size),
+            *pair(rows),
+            *pair(CHUNKS, rows),
+            *pair(CHUNKS, rows),
+            *pair(CHUNKS, group),
+            *pair(CHUNKS, group),
+            *pair(CHUNKS, rows),
+        ],
+        compiler_params=pltpu.CompilerParams(collective_id=1, has_side_effects=True, vmem_limit_bytes=VMEM_LIMIT),
+        name="experts",
+    )(head_output, meta, residual, norm_gain.reshape(1, model), out_weight, shared_gate, shared_up, shared_down,
+      expert_gate, expert_up, expert_down)
 
 
 def body(
@@ -264,21 +569,9 @@
     route_weights,
 ):
     head_output = attention(queries, key_heads, value_heads, head_gain)
-    token_heads = lax.all_to_all(head_output, "tp", split_axis=0, concat_axis=1, tiled=True)
-    branch = jnp.dot(token_heads, out_weight, preferred_element_type=jnp.float32)
-    stream = (residual.astype(jnp.float32) + branch).astype(jnp.bfloat16)
-    stream_wide = stream.astype(jnp.float32)
-    inverse = lax.rsqrt(jnp.mean(stream_wide * stream_wide, axis=1, keepdims=True) + EPSILON)
-    expert_input = (stream_wide * inverse * norm_gain).astype(jnp.bfloat16)
-    shared_hidden = (
-        jax.nn.silu(jnp.dot(expert_input, shared_gate, preferred_element_type=jnp.float32))
-        * jnp.dot(expert_input, shared_up, preferred_element_type=jnp.float32)
-    ).astype(jnp.bfloat16)
-    shared_term = jnp.dot(shared_hidden, shared_down, preferred_element_type=jnp.float32)
-    routed = routed_sum(
-        expert_input, expert_gate, expert_up, expert_down, routed_experts, route_weights
-    )
-    return (stream_wide + shared_term + routed).astype(jnp.bfloat16)
+    return experts(
+        head_output, residual, out_weight, norm_gain, shared_gate, shared_up, shared_down, expert_gate, expert_up, expert_down,
+        routed_experts, route_weights)
 
 
 def solution(mesh):

time: 242 us -> 162 us (0.67)
  Pallas kernels: 10.7 us -> 156 us
  waiting for transfers between devices: 142 us -> 0 us
  starting transfers between devices: 39 us -> 0 us
  matrix products: 34.2 us -> 0 us
  other arithmetic: 9.39 us -> 3.64 us
  local copies, waits for them, and re-layouts: 6.83 us -> 1.88 us
    pallas_call x0 -> x1, Pallas kernels: none -> 145 us  [experts(): pl.pallas_call(functools.partial(moe_kernel, rows, capacity, span), out_s...]
    all_to_all x3 -> x0, waiting for transfers between devices: 142 us -> none  [the longest x1 70.9 us: routed_sum(): lax.all_to_all(outgoing, ('sp', 'tp'), split_axis=0, concat_axis=0, tiled...]
    all_to_all x3 -> x0, starting transfers between devices: 39 us -> none  [the longest x1 30.9 us: routed_sum(): lax.all_to_all(outgoing, ('sp', 'tp'), split_axis=0, concat_axis=0, tiled...]
    dot_general x10 -> x0, matrix products: 34.2 us -> none  [the longest x2 13.9 us: routed_sum(): jnp.dot(hidden, expert_down[expert], preferred_element_type=jnp.float32)]
    select_n x1 -> x0, other arithmetic: 5.17 us -> none  [routed_sum(): result = jnp.where(mine, down, result)]
    slice x1 -> x0, local copies, waits for them, and re-layouts: 2.88 us -> none  [routed_sum(): grouped = arrived[:, first:last].reshape(-1, model_width)]
  transfers between devices with their start and end apart: 3 -> 0, of which waited for: 3 -> 0; matrix products, arithmetic and copies ran while one was open for 2% -> 0% of each run, Pallas kernels for 0% -> 0%
where the time goes in v1:
time: 162 us; the launch traced here: 161 us
  Pallas kernels  156 us (96%)
  other arithmetic  3.64 us (2%)
  local copies, waits for them, and re-layouts  1.88 us (1%)
    pallas_call x1, Pallas kernels, experts(): pl.pallas_call(functools.partial(moe_kernel, rows, capacity, span), out_s...  145 us
    pallas_call x1, Pallas kernels, attention(): pl.pallas_call(functools.partial(attention_kernel, rows), out_shape=jax.S...  10.6 us

profile of v1, /device:TPU:0, one launch (start us, length us, event | category | flops | bytes accessed | tf_op | source)
XLA Modules:
  0.0 161.3 jit_solution(8927064427126733695)
XLA Ops:
  0.0 0.7 convert_bitcast_fusion
  0.7 1.3 pad_maximum_fusion.1.meta_ref
  1.9 1.7 %pad_maximum_fusion.kv_ref = bf16[512,256]{1,0:T(8,128)(2,1)} fusion(bf16[512,128]{1,0:T(8,128)(2,1)} %param.17, bf16[512,128]{1,0:T(8,128)(2,1)} %param.16), kind=kLoop, calls=%fused_computation | loop fusion | flops 524288 | bytes 524288 | tf_op jit(solution)/shard_map/concatenate | solution.py:176
  3.6 10.6 %attention.1.heads_ref = bf16[512,128]{1,0:T(8,128)(2,1)} custom-call(bf16[512,128]{1,0:T(8,128)(2,1)} %q_ref.1, bf16[512,256]{1,0:T(8,128)(2,1)} %pad_maximum_fusion.kv_ref, f32[1,128]{1,0:T(1,128)} %bitcast.7), custom_call_target="tpu_custom_call" | custom-call | tf_op jit(solution)/shard_map/attention/pallas_call | solution.py:178
  14.3 145.1 %experts.1 = bf16[128,2048]{1,0:T(8,128)(2,1)} custom-call(bf16[512,128]{1,0:T(8,128)(2,1)} %attention.1.heads_ref, f32[8,128]{1,0:T(8,128)} %pad_maximum_fusion.1.meta_ref, bf16[128,2048]{1,0:T(8,128)(2,1)} %residual_ref.1, f32[1,2048]{1,0:T(1,128)} %bitcast.5, bf16[512,2048]{1,0:T(8,128)(2,1)} %out_weight.1, bf16[2048,512]{1,0:T(8,128)(2,1)} %shared_gate.1, ...), custom_call_target="tpu_custom_call" | custom-call | tf_op jit(solution)/shard_map/experts/pallas_call | solution.py:511
  159.4 1.9 %copy.17 = bf16[128,2048]{1,0:T(8,128)(2,1)} copy(bf16[128,2048]{1,0:T(8,128)(2,1)} %experts.1) | data formatting | bytes 1048576

commit v2 on v1

--- a/solution.py
+++ b/solution.py
@@ -18,7 +18,9 @@
 LOG2E = 1.4426950408889634
 MESH = pl.DeviceIdType.MESH
 CHUNKS = 8
+FIRST = 3
 LAG = 2
+PACK = 16
 VMEM_LIMIT = 67043328
 
 
@@ -201,19 +203,27 @@
 
 def moe_kernel(
     rows, capacity, span, heads_ref, meta_ref, residual_ref, gain_ref, out_weight, shared_gate, shared_up, shared_down, expert_gate,
-    expert_up, expert_down, out_ref, head_rows, meta_all, slots, place, mix, inputs, gathered, outgoing, arrived, returned, landed, base,
-    gate_sum, up_sum, hidden, w_out, w_sgate, w_sup, w_sdown, w_gate, w_up, w_down, w_sem, head_send, head_recv, meta_send, meta_recv,
-    up_send, up_recv, down_send, down_recv, go_send, go_recv, back_send, back_recv, part_send, part_recv):
+    expert_up, expert_down, out_ref, head_rows, meta_all, slots, place, mix, inputs, gathered, outgoing, arrived, returned, chained, landed,
+    base, gate_sum, up_sum, hidden, w_out, w_sgate, w_sup, w_sdown, w_gate, w_up, w_down, w_sem, head_send, head_recv, meta_send,
+    meta_recv, up_send, up_recv, down_send, down_recv, go_send, go_recv, back_send, back_recv, near_send, near_recv, chain_send,
+    chain_recv, far_send, far_recv):
     me = lax.axis_index("sp")
     tp = lax.axis_index("tp")
     row, col = me // COLUMNS, me % COLUMNS
     tp_size = head_rows.shape[0]
     group = COLUMNS * tp_size
     mine = col * tp_size + tp
-    chunks, _, local, _, width = outgoing.shape
+    _, chunks, _, block_rows, width = outgoing.shape
+    local = gate_sum.shape[0]
     count = residual_ref.shape[0]
     picks = meta_ref.shape[0] // 2
-    total = group * local * span
+    total = group * block_rows
+    reach = rows // 2
+    half = row // reach
+    near_first, far_first = half * reach, (1 - half) * reach
+    outward = (1 - half) * (reach - 1 - row) + half * (row - reach)
+    inner_row = row + 1 - 2 * half
+    bounds = [(e * span // PACK * PACK, round_up((e + 1) * span, PACK)) for e in range(local)]
 
     loads = []
     for index, (source, target) in enumerate((
@@ -255,28 +265,201 @@
         meta_copy((row + step) % rows, row).start()
     head_rows[tp] = heads_ref[pl.ds(pl.multiple_of(tp * count, count), count), :]
     meta_all[row] = meta_ref[...]
+
+    def up_copy(chunk, block):
+        return pltpu.make_async_remote_copy(
+            src_ref=gathered.at[chunk, block], dst_ref=gathered.at[chunk, block], send_sem=up_send.at[chunk, block],
+            recv_sem=up_recv.at[chunk, block], device_id=device(row + 1, col, tp), device_id_type=MESH)
+
+    def down_copy(chunk, block):
+        return pltpu.make_async_remote_copy(
+            src_ref=gathered.at[chunk, block], dst_ref=gathered.at[chunk, block], send_sem=down_send.at[chunk, block],
+            recv_sem=down_recv.at[chunk, block], device_id=device(row - 1, col, tp), device_id_type=MESH)
+
+    def from_below(chunk, block):
+        up_copy(chunk, block).wait_recv()
+
+        @pl.when(row < rows - 1)
+        def _():
+            up_copy(chunk, block).start()
+
+    def from_above(chunk, block):
+        down_copy(chunk, block).wait_recv()
+
+        @pl.when(row > 0)
+        def _():
+            down_copy(chunk, block).start()
+
+    def gather_near(chunk):
+        for depth in range(1, reach):
+            @pl.when(row - depth >= near_first)
+            def _():
+                from_below(chunk, row - depth)
+
+            @pl.when(row + depth < near_first + reach)
+            def _():
+                from_above(chunk, row + depth)
+
+    def gather_far(chunk):
+        for depth in range(1, rows):
+            @pl.when((row - depth >= 0) & (row - depth < near_first))
+            def _():
+                from_below(chunk, row - depth)
+
+            @pl.when((row + depth >= near_first + reach) & (row + depth < rows))
+            def _():
+                from_above(chunk, row + depth)
+
+    def go_copy(part, chunk, peer, source):
+        at_col, at_tp = peer
+        return pltpu.make_async_remote_copy(
+            src_ref=outgoing.at[part, chunk, at_col * tp_size + at_tp], dst_ref=arrived.at[part, chunk, source],
+            send_sem=go_send.at[part, chunk, at_col * tp_size + at_tp], recv_sem=go_recv.at[part, chunk, source],
+            device_id=device(row, at_col, at_tp), device_id_type=MESH)
+
+    def back_copy(part, chunk, peer, source):
+        at_col, at_tp = peer
+        return pltpu.make_async_remote_copy(
+            src_ref=outgoing.at[part, chunk, at_col * tp_size + at_tp], dst_ref=returned.at[part, chunk, source],
+            send_sem=back_send.at[part, chunk, at_col * tp_size + at_tp], recv_sem=back_recv.at[part, chunk, source],
+            device_id=device(row, at_col, at_tp), device_id_type=MESH)
+
+    def near_copy(chunk, block, source):
+        return pltpu.make_async_remote_copy(
+            src_ref=gathered.at[chunk, block], dst_ref=landed.at[chunk, source - near_first],
+            send_sem=near_send.at[chunk, block - near_first], recv_sem=near_recv.at[chunk, source - near_first],
+            device_id=device(block, col, tp), device_id_type=MESH)
+
+    def chain_copy(chunk, index):
+        return pltpu.make_async_remote_copy(
+            src_ref=gathered.at[chunk, far_first + index], dst_ref=chained.at[chunk, index],
+            send_sem=chain_send.at[chunk, index], recv_sem=chain_recv.at[chunk, index],
+            device_id=device(inner_row, col, tp), device_id_type=MESH)
+
+    def far_copy(chunk, index):
+        return pltpu.make_async_remote_copy(
+            src_ref=gathered.at[chunk, far_first + index], dst_ref=landed.at[chunk, reach],
+            send_sem=far_send.at[chunk, index], recv_sem=far_recv.at[chunk],
+            device_id=device(far_first + index, col, tp), device_id_type=MESH)
+
+    def dispatch(part, chunk):
+        first_block = near_first if part == 0 else far_first
+        tokens = gathered[chunk, pl.ds(first_block, reach)].reshape(reach * count, width)
+        rows_out = jnp.dot(place[part], tokens, preferred_element_type=jnp.float32).astype(jnp.bfloat16)
+        outgoing[part, chunk] = rows_out.reshape(group, block_rows, width)
+        arrived[part, chunk, mine] = outgoing[part, chunk, mine]
+        for peer in peers:
+            go_copy(part, chunk, peer, mine).start()
+
+    def enter(part, chunk):
+        for peer in peers:
+            go_copy(part, chunk, peer, peer[0] * tp_size + peer[1]).wait_recv()
+        deep = pl.ds(pl.multiple_of(chunk * width, width), width)
+        for expert, (low, high) in enumerate(bounds):
+            block = arrived[part, chunk, :, low:high, :].reshape(group * (high - low), width)
+            gate_sum[expert] += jnp.dot(block, w_gate[expert, deep, :], preferred_element_type=jnp.float32)
+            up_sum[expert] += jnp.dot(block, w_up[expert, deep, :], preferred_element_type=jnp.float32)
+
+    def activate(part):
+        for expert in range(local):
+            gate = gate_sum[expert]
+            hidden[part, expert] = (gate / (1.0 + jnp.exp(-gate)) * up_sum[expert]).astype(jnp.bfloat16)
+
+    def leave(part, chunk):
+        for peer in peers:
+            go_copy(part, chunk, peer, mine).wait_send()
+        wide = pl.ds(pl.multiple_of(chunk * width, width), width)
+        downs = [
+            jnp.dot(hidden[part, expert], w_down[expert, :, wide], preferred_element_type=jnp.float32).reshape(group, high - low, width)
+            for expert, (low, high) in enumerate(bounds)]
+        inside = lax.broadcasted_iota(jnp.int32, (1, PACK, 1), 1)
+        for tile in range(0, block_rows, PACK):
+            value = None
+            for expert, (low, high) in enumerate(bounds):
+                if low <= tile < high:
+                    piece = downs[expert][:, tile - low : tile - low + PACK, :]
+                    value = piece if value is None else jnp.where(inside + tile >= expert * span, piece, value)
+            outgoing[part, chunk, :, tile : tile + PACK, :] = value.astype(jnp.bfloat16)
+        returned[part, chunk, mine] = outgoing[part, chunk, mine]
+        for peer in peers:
+            back_copy(part, chunk, peer, mine).start()
+
+    def combine(part, chunk):
+        for peer in peers:
+            back_copy(part, chunk, peer, peer[0] * tp_size + peer[1]).wait_recv()
+        return returned[part, chunk].reshape(total, width)
+
+    def combine_near(chunk):
+        results = combine(0, chunk)
+        for step in range(1, reach):
+            block = near_first + (row - near_first + step) % reach
+            gathered[chunk, block] = jnp.dot(mix[block], results, preferred_element_type=jnp.float32).astype(jnp.bfloat16)
+        base[chunk] += jnp.dot(mix[row], results, preferred_element_type=jnp.float32)
+        for step in range(1, reach):
+            near_copy(chunk, near_first + (row - near_first + step) % reach, row).start()
+
+    def combine_far(chunk):
+        results = combine(1, chunk)
+        for index in range(reach):
+            block = far_first + index
+            gathered[chunk, block] = jnp.dot(mix[block], results, preferred_element_type=jnp.float32).astype(jnp.bfloat16)
+
+        @pl.when(outward == reach - 1)
+        def _():
+            onward(chunk)
+
+    def onward(chunk):
+        for index in range(reach):
+            @pl.when(outward > 0)
+            def _():
+                chain_copy(chunk, index).start()
+
+            @pl.when(outward == 0)
+            def _():
+                far_copy(chunk, index).start()
+
+    def fold(chunk):
+        @pl.when(outward < reach - 1)
+        def _():
+            for index in range(reach):
+                chain_copy(chunk, index).wait_recv()
+                block = far_first + index
+                gathered[chunk, block] = (
+                    gathered[chunk, block].astype(jnp.float32) + chained[chunk, index].astype(jnp.float32)).astype(jnp.bfloat16)
+            onward(chunk)
+
+    def loop(first, last, step):
+        def one(index, unused):
+            step(index)
+            return unused
+
+        lax.fori_loop(first, last, one, 0)
+
     for step in range(1, rows):
         meta_copy((row + step) % rows, (row + step) % rows).wait_recv()
-
     expert_place = lax.broadcasted_iota(jnp.int32, (group * local, count), 0).astype(jnp.float32)
     slot_place = lax.broadcasted_iota(jnp.int32, (total, count), 0).astype(jnp.float32)
-    first = lax.broadcasted_iota(jnp.int32, (count, count), 0)
-    second = lax.broadcasted_iota(jnp.int32, (count, count), 1)
-    earlier = (first < second).astype(jnp.bfloat16)
+    before = lax.broadcasted_iota(jnp.int32, (count, count), 0)
+    after = lax.broadcasted_iota(jnp.int32, (count, count), 1)
+    earlier = (before < after).astype(jnp.bfloat16)
     lowest = (row * (group * local)).astype(jnp.float32)
-    for block in range(rows):
-        meta = meta_all[block]
-        chosen = [meta[k : k + 1, :] - lowest for k in range(picks)]
-        tables = [jnp.where(expert_place == chosen[k], 1.0, 0.0) for k in range(picks)]
-        tally = jnp.dot(sum(tables).astype(jnp.bfloat16), earlier, preferred_element_type=jnp.float32)
-        placed = jnp.zeros((total, count), jnp.float32)
-        for k in range(picks):
-            ranking = jnp.sum(tables[k] * tally, axis=0, keepdims=True)
-            inside = (chosen[k] >= 0.0) & (chosen[k] < float(group * local))
-            slot = jnp.where(inside, chosen[k] * float(span) + (block * capacity + ranking), -1.0)
-            slots[block, k : k + 1, :] = slot
-            placed = jnp.where(slot_place == slot, 1.0, placed)
-        place[:, block * count : (block + 1) * count] = placed.astype(jnp.bfloat16)
+    for part in range(2):
+        for index in range(reach):
+            block = (near_first if part == 0 else far_first) + index
+            meta = meta_all[block]
+            chosen = [meta[k : k + 1, :] - lowest for k in range(picks)]
+            tables = [jnp.where(expert_place == chosen[k], 1.0, 0.0) for k in range(picks)]
+            tally = jnp.dot(sum(tables).astype(jnp.bfloat16), earlier, preferred_element_type=jnp.float32)
+            placed = jnp.zeros((total, count), jnp.float32)
+            for k in range(picks):
+                ranking = jnp.sum(tables[k] * tally, axis=0, keepdims=True)
+                inside = (chosen[k] >= 0.0) & (chosen[k] < float(group * local))
+                owner = jnp.floor(chosen[k] * (1.0 / local))
+                start = owner * float(block_rows) + (chosen[k] - owner * float(local)) * float(span)
+                slot = jnp.where(inside, start + (index * capacity + ranking), -1.0)
+                slots[block, k : k + 1, :] = slot
+                placed = jnp.where(slot_place == slot, 1.0, placed)
+            place[part, :, index * count : (index + 1) * count] = placed.astype(jnp.bfloat16)
 
     loads[0].wait()
     for step in range(1, tp_size):
@@ -292,16 +475,6 @@
         base[chunk] = stream[:, columns]
         gathered[chunk, row] = normed[:, columns]
 
-    def up_copy(chunk, block):
-        return pltpu.make_async_remote_copy(
-            src_ref=gathered.at[chunk, block], dst_ref=gathered.at[chunk, block], send_sem=up_send.at[chunk, block],
-            recv_sem=up_recv.at[chunk, block], device_id=device(row + 1, col, tp), device_id_type=MESH)
-
-    def down_copy(chunk, block):
-        return pltpu.make_async_remote_copy(
-            src_ref=gathered.at[chunk, block], dst_ref=gathered.at[chunk, block], send_sem=down_send.at[chunk, block],
-            recv_sem=down_recv.at[chunk, block], device_id=device(row - 1, col, tp), device_id_type=MESH)
-
     def send_own(chunk):
         @pl.when(row < rows - 1)
         def _():
@@ -311,110 +484,36 @@
         def _():
             down_copy(chunk, row).start()
 
-    def gather(chunk):
-        for depth in range(1, rows):
-            @pl.when(row >= depth)
-            def _():
-                up_copy(chunk, row - depth).wait_recv()
-
-                @pl.when(row < rows - 1)
-                def _():
-                    up_copy(chunk, row - depth).start()
-
-            @pl.when(row + depth < rows)
-            def _():
-                down_copy(chunk, row + depth).wait_recv()
-
-                @pl.when(row > 0)
-                def _():
-                    down_copy(chunk, row + depth).start()
-
-    def go_copy(chunk, peer, source):
-        at_col, at_tp = peer
-        return pltpu.make_async_remote_copy(
-            src_ref=outgoing.at[chunk, at_col * tp_size + at_tp], dst_ref=arrived.at[chunk, :, source],
-            send_sem=go_send.at[chunk, at_col * tp_size + at_tp], recv_sem=go_recv.at[chunk, source],
-            device_id=device(row, at_col, at_tp), device_id_type=MESH)
-
-    def back_copy(chunk, peer, source):
-        at_col, at_tp = peer
-        return pltpu.make_async_remote_copy(
-            src_ref=outgoing.at[chunk, at_col * tp_size + at_tp], dst_ref=returned.at[chunk, source],
-            send_sem=back_send.at[chunk, at_col * tp_size + at_tp], recv_sem=back_recv.at[chunk, source],
-            device_id=device(row, at_col, at_tp), device_id_type=MESH)
-
-    def part_copy(chunk, block, source):
-        return pltpu.make_async_remote_copy(
-            src_ref=gathered.at[chunk, block], dst_ref=landed.at[chunk, source], send_sem=part_send.at[chunk, block],
-            recv_sem=part_recv.at[chunk, source], device_id=device(block, col, tp), device_id_type=MESH)
-
-    def dispatch(chunk):
-        tokens = gathered[chunk].reshape(rows * count, width)
-        rows_out = jnp.dot(place[...], tokens, preferred_element_type=jnp.float32).astype(jnp.bfloat16)
-        outgoing[chunk] = rows_out.reshape(group, local, span, width)
-        arrived[chunk, :, mine] = outgoing[chunk, mine]
-        for peer in peers:
-            go_copy(chunk, peer, mine).start()
-
-    def enter(chunk):
-        for peer in peers:
-            go_copy(chunk, peer, peer[0] * tp_size + peer[1]).wait_recv()
-        deep = pl.ds(pl.multiple_of(chunk * width, width), width)
-        for expert in range(local):
-            block = arrived[chunk, expert].reshape(group * span, width)
-            gate_sum[expert] += jnp.dot(block, w_gate[expert, deep, :], preferred_element_type=jnp.float32)
-            up_sum[expert] += jnp.dot(block, w_up[expert, deep, :], preferred_element_type=jnp.float32)
-
-    for chunk in range(min(2, chunks)):
-        send_own(chunk)
+    loop(0, chunks, send_own)
     gate_sum[...] = jnp.zeros_like(gate_sum)
     up_sum[...] = jnp.zeros_like(up_sum)
+
+    def near_step(chunk):
+        gather_near(chunk)
+        dispatch(0, chunk)
+
+    loop(0, chunks, near_step)
     loads[1].wait()
     loads[2].wait()
 
-    def forward(index, unused):
-        @pl.when(index < chunks)
-        def _():
-            gather(index)
-
-            @pl.when(index + 2 < chunks)
-            def _():
-                send_own(index + 2)
-
-            dispatch(index)
-
-        @pl.when(index >= LAG)
-        def _():
-            enter(index - LAG)
-
-        return unused
-
-    lax.fori_loop(0, chunks + LAG, forward, 0)
-
-    for expert in range(local):
-        gate = gate_sum[expert]
-        hidden[expert] = (gate / (1.0 + jnp.exp(-gate)) * up_sum[expert]).astype(jnp.bfloat16)
-
-    def sent(chunk, unused):
-        for peer in peers:
-            go_copy(chunk, peer, mine).wait_send()
-        return unused
-
-    lax.fori_loop(0, chunks, sent, 0)
+    def far_step(chunk):
+        gather_far(chunk)
+        dispatch(1, chunk)
+        enter(0, chunk)
+
+    loop(0, chunks, far_step)
+    activate(0)
     loads[3].wait()
-
-    def leave(chunk, unused):
-        wide = pl.ds(pl.multiple_of(chunk * width, width), width)
-        for expert in range(local):
-            down = jnp.dot(hidden[expert], w_down[expert, :, wide], preferred_element_type=jnp.float32).astype(jnp.bfloat16)
-            outgoing[chunk, :, expert] = down.reshape(group, span, width)
-        returned[chunk, mine] = outgoing[chunk, mine]
-        for peer in peers:
-            back_copy(chunk, peer, mine).start()
-        return unused
-
-    lax.fori_loop(0, chunks, leave, 0)
-
+    loop(0, FIRST, lambda chunk: leave(0, chunk))
+
+    for load in loads[4:]:
+        load.wait()
+    x = inputs[...]
+    shared = jnp.dot(x, w_sgate[...], preferred_element_type=jnp.float32)
+    shared = (shared / (1.0 + jnp.exp(-shared)) * jnp.dot(x, w_sup[...], preferred_element_type=jnp.float32)).astype(jnp.bfloat16)
+    for chunk in range(chunks):
+        columns = slice(chunk * width, (chunk + 1) * width)
+        base[chunk] += jnp.dot(shared, w_sdown[:, columns], preferred_element_type=jnp.float32)
     for block in range(rows):
         weighed = jnp.zeros((total, count), jnp.float32)
         for k in range(picks):
@@ -422,64 +521,71 @@
             weighed = jnp.where(slot_place == slot, meta_all[block, picks + k : picks + k + 1, :], weighed)
         mix[block] = weighed.T.astype(jnp.bfloat16)
 
-    for load in loads[4:]:
-        load.wait()
-
-    def gathered_sent(chunk, unused):
+    gate_sum[...] = jnp.zeros_like(gate_sum)
+    up_sum[...] = jnp.zeros_like(up_sum)
+    loop(0, chunks, lambda chunk: enter(1, chunk))
+    activate(1)
+    loop(0, chunks, lambda chunk: leave(1, chunk))
+    loop(FIRST, chunks, lambda chunk: leave(0, chunk))
+
+    def gathered_sent(chunk):
         @pl.when(row < rows - 1)
         def _():
-            def one(block, inner):
-                up_copy(chunk, block).wait_send()
-                return inner
-
-            lax.fori_loop(0, row + 1, one, 0)
+            loop(0, row + 1, lambda block: up_copy(chunk, block).wait_send())
 
         @pl.when(row > 0)
         def _():
-            def one(block, inner):
-                down_copy(chunk, block).wait_send()
-                return inner
-
-            lax.fori_loop(row, rows, one, 0)
-
-        return unused
-
-    lax.fori_loop(0, chunks, gathered_sent, 0)
-    x = inputs[...]
-    shared = jnp.dot(x, w_sgate[...], preferred_element_type=jnp.float32)
-    shared = (shared / (1.0 + jnp.exp(-shared)) * jnp.dot(x, w_sup[...], preferred_element_type=jnp.float32)).astype(jnp.bfloat16)
-    for chunk in range(chunks):
-        columns = slice(chunk * width, (chunk + 1) * width)
-        base[chunk] += jnp.dot(shared, w_sdown[:, columns], preferred_element_type=jnp.float32)
-
-    def combine(chunk, unused):
+            loop(row, rows, lambda block: down_copy(chunk, block).wait_send())
+
+    loop(0, chunks, gathered_sent)
+    loop(0, FIRST, combine_near)
+
+    def far_back(index):
+        combine_far(index)
+
+        @pl.when(index >= LAG)
+        def _():
+            fold(index - LAG)
+
+    loop(0, chunks, far_back)
+
+    def near_back(index):
+        combine_near(index)
+
+        @pl.when(index - FIRST < LAG)
+        def _():
+            fold(index - FIRST + chunks - LAG)
+
+    loop(FIRST, chunks, near_back)
+
+    def close(chunk):
+        value = base[chunk]
+        far_copy(chunk, 0).wait_recv()
+        value += landed[chunk, reach].astype(jnp.float32)
+        for step in range(1, reach):
+            source = near_first + (row - near_first + step) % reach
+            near_copy(chunk, source, source).wait_recv()
+            value += landed[chunk, source - near_first].astype(jnp.float32)
+        out_ref[:, pl.ds(pl.multiple_of(chunk * width, width), width)] = value.astype(out_ref.dtype)
+
+    loop(0, chunks, close)
+
+    def settle(chunk):
         for peer in peers:
-            back_copy(chunk, peer, peer[0] * tp_size + peer[1]).wait_recv()
-        results = returned[chunk].reshape(total, width)
-        for step in range(1, rows):
-            block = (row + step) % rows
-            gathered[chunk, block] = jnp.dot(mix[block], results, preferred_element_type=jnp.float32).astype(jnp.bfloat16)
-        base[chunk] += jnp.dot(mix[row], results, preferred_element_type=jnp.float32)
-        for step in range(1, rows):
-            part_copy(chunk, (row + step) % rows, row).start()
-        return unused
-
-    lax.fori_loop(0, chunks, combine, 0)
-
-    def close(chunk, unused):
-        value = base[chunk]
-        for step in range(1, rows):
-            source = (row + step) % rows
-            part_copy(chunk, source, source).wait_recv()
-            value += landed[chunk, source].astype(jnp.float32)
-        out_ref[:, pl.ds(pl.multiple_of(chunk * width, width), width)] = value.astype(out_ref.dtype)
-        for peer in peers:
-            back_copy(chunk, peer, mine).wait_send()
-        for step in range(1, rows):
-            part_copy(chunk, (row + step) % rows, row).wait_send()
-        return unused
-
-    lax.fori_loop(0, chunks, close, 0)
+            back_copy(0, chunk, peer, mine).wait_send()
+            back_copy(1, chunk, peer, mine).wait_send()
+        for step in range(1, reach):
+            near_copy(chunk, near_first + (row - near_first + step) % reach, row).wait_send()
+        for index in range(reach):
+            @pl.when(outward > 0)
+            def _():
+                chain_copy(chunk, index).wait_send()
+
+            @pl.when(outward == 0)
+            def _():
+                far_copy(chunk, index).wait_send()
+
+    loop(0, chunks, settle)
     for step in range(1, tp_size):
         head_copy((tp + step) % tp_size, tp).wait_send()
     for step in range(1, rows):
@@ -493,12 +599,14 @@
     model = residual.shape[1]
     sp_size, tp_size = lax.axis_size("sp"), lax.axis_size("tp")
     rows, group = sp_size // COLUMNS, COLUMNS * tp_size
+    reach = rows // 2
     local, _, inner = expert_gate.shape
-    shared_inner = shared_gate.shape[1]
     expert_count = local * sp_size * tp_size
     capacity = max(2, 3 * count * picks // (2 * expert_count))
-    span = round_up(rows * capacity, 16)
-    total = group * local * span
+    span = round_up(reach * capacity, 8)
+    block_rows = round_up(local * span, PACK)
+    total = group * block_rows
+    wide = max(round_up((e + 1) * span, PACK) - e * span // PACK * PACK for e in range(local))
     width = model // CHUNKS
     meta = jnp.concatenate([routed_experts.astype(jnp.float32).T, route_weights.T], axis=0)
     vmem = pl.BlockSpec(memory_space=pltpu.VMEM)
@@ -517,18 +625,19 @@
             pltpu.VMEM((tp_size, count, head_output.shape[1]), half),
             pltpu.VMEM((rows, 2 * picks, count), jnp.float32),
             pltpu.VMEM((rows, 2 * picks, count), jnp.float32),
-            pltpu.VMEM((total, rows * count), half),
+            pltpu.VMEM((2, total, reach * count), half),
             pltpu.VMEM((rows, count, total), half),
             pltpu.VMEM((count, model), half),
             pltpu.VMEM((CHUNKS, rows, count, width), half),
-            pltpu.VMEM((CHUNKS, group, local, span, width), half),
-            pltpu.VMEM((CHUNKS, local, group, span, width), half),
-            pltpu.VMEM((CHUNKS, group, local, span, width), half),
-            pltpu.VMEM((CHUNKS, rows, count, width), half),
+            pltpu.VMEM((2, CHUNKS, group, block_rows, width), half),
+            pltpu.VMEM((2, CHUNKS, group, block_rows, width), half),
+            pltpu.VMEM((2, CHUNKS, group, block_rows, width), half),
+            pltpu.VMEM((CHUNKS, reach, count, width), half),
+            pltpu.VMEM((CHUNKS, reach + 1, count, width), half),
             pltpu.VMEM((CHUNKS, count, width), jnp.float32),
-            pltpu.VMEM((local, group * span, inner), jnp.float32),
-            pltpu.VMEM((local, group * span, inner), jnp.float32),
-            pltpu.VMEM((local, group * span, inner), half),
+            pltpu.VMEM((local, group * wide, inner), jnp.float32),
+            pltpu.VMEM((local, group * wide, inner), jnp.float32),
+            pltpu.VMEM((2, local, group * wide, inner), half),
             pltpu.VMEM(out_weight.shape, half),
             pltpu.VMEM(shared_gate.shape, half),
             pltpu.VMEM(shared_up.shape, half),
@@ -541,9 +650,12 @@
             *pair(rows),
             *pair(CHUNKS, rows),
             *pair(CHUNKS, rows),
-            *pair(CHUNKS, group),
-            *pair(CHUNKS, group),
-            *pair(CHUNKS, rows),
+            *pair(2, CHUNKS, group),
+            *pair(2, CHUNKS, group),
+            *pair(CHUNKS, reach),
+            *pair(CHUNKS, reach),
+            pltpu.SemaphoreType.DMA((CHUNKS, reach)),
+            pltpu.SemaphoreType.DMA((CHUNKS,)),
         ],
         compiler_params=pltpu.CompilerParams(collective_id=1, has_side_effects=True, vmem_limit_bytes=VMEM_LIMIT),
         name="experts",

time: 162 us -> 145 us (0.90)
  Pallas kernels: 156 us -> 139 us
    pallas_call x1, Pallas kernels: 145 us -> 128 us  [experts(): pl.pallas_call(functools.partial(moe_kernel, rows, capacity, span), out_s...]
where the time goes in v2:
time: 145 us
  Pallas kernels  139 us (96%)
  other arithmetic  3.64 us (3%)
  local copies, waits for them, and re-layouts  1.88 us (1%)
    pallas_call x1, Pallas kernels, experts(): pl.pallas_call(functools.partial(moe_kernel, rows, capacity, span), out_s...  128 us
    pallas_call x1, Pallas kernels, attention(): pl.pallas_call(functools.partial(attention_kernel, rows), out_shape=jax.S...  10.6 us

profile of v2, /device:TPU:0, one launch (start us, length us, event | category | flops | bytes accessed | tf_op | source)
XLA Modules:
  0.0 144.7 jit_solution(4885286435716475856)
XLA Ops:
  0.0 0.7 convert_bitcast_fusion
  0.7 1.3 pad_maximum_fusion.1.meta_ref
  1.9 1.7 %pad_maximum_fusion.kv_ref = bf16[512,256]{1,0:T(8,128)(2,1)} fusion(bf16[512,128]{1,0:T(8,128)(2,1)} %param.17, bf16[512,128]{1,0:T(8,128)(2,1)} %param.16), kind=kLoop, calls=%fused_computation | loop fusion | flops 524288 | bytes 524288 | tf_op jit(solution)/shard_map/concatenate | solution.py:178
  3.6 10.6 %attention.1.heads_ref = bf16[512,128]{1,0:T(8,128)(2,1)} custom-call(bf16[512,128]{1,0:T(8,128)(2,1)} %q_ref.1, bf16[512,256]{1,0:T(8,128)(2,1)} %pad_maximum_fusion.kv_ref, f32[1,128]{1,0:T(1,128)} %bitcast.7), custom_call_target="tpu_custom_call" | custom-call | tf_op jit(solution)/shard_map/attention/pallas_call | solution.py:180
  14.3 128.5 %experts.1 = bf16[128,2048]{1,0:T(8,128)(2,1)} custom-call(bf16[512,128]{1,0:T(8,128)(2,1)} %attention.1.heads_ref, f32[8,128]{1,0:T(8,128)} %pad_maximum_fusion.1.meta_ref, bf16[128,2048]{1,0:T(8,128)(2,1)} %residual_ref.1, f32[1,2048]{1,0:T(1,128)} %bitcast.5, bf16[512,2048]{1,0:T(8,128)(2,1)} %out_weight.1, bf16[2048,512]{1,0:T(8,128)(2,1)} %shared_gate.1, ...), custom_call_target="tpu_custom_call" | custom-call | tf_op jit(solution)/shard_map/experts/pallas_call | solution.py:619
  142.8 1.9 %copy.17 = bf16[128,2048]{1,0:T(8,128)(2,1)} copy(bf16[128,2048]{1,0:T(8,128)(2,1)} %experts.1) | data formatting | bytes 1048576

commit v3 on v2

v3 whole, which is shorter than its diff:
```python
import functools
import math

import jax
import jax.numpy as jnp
from jax import lax
from jax.experimental import pallas as pl
from jax.experimental.pallas import tpu as pltpu
from jax.sharding import PartitionSpec as P

HEAD_DIM = 64


EPSILON = 1e-06

COLUMNS = 2
TILE = 256
LOG2E = 1.4426950408889634
MESH = pl.DeviceIdType.MESH
CHUNKS = 8
FIRST = 2
LAG = 3
AHEAD = 3
PACK = 16
VMEM_LIMIT = 67043328


def attention_step(rows, q_ref, kv_ref, gain_ref, out_ref, held, masked, acc, carry, up_send, up_recv, side_send, side_recv):
    me = lax.axis_index("sp")
    row, col = me // COLUMNS, me % COLUMNS
    seq, width = q_ref.shape
    heads = width // HEAD_DIM
    tile = min(TILE, seq)
    tiles = seq // tile
    other = row * COLUMNS + (COLUMNS - 1 - col)

    def up_copy(source, depth, piece):
        place = (row - depth) * COLUMNS + col
        part = pl.ds(piece * tile, tile)
        return pltpu.make_async_remote_copy(
            src_ref=source.at[part, :], dst_ref=held.at[place, part, :], send_sem=up_send.at[depth, piece],
            recv_sem=up_recv.at[depth, piece], device_id={"sp": me + COLUMNS}, device_id_type=MESH)

    def side_copy(source, depth, piece):
        place = (row - depth) * COLUMNS + col
        part = pl.ds(piece * tile, tile)
        return pltpu.make_async_remote_copy(
            src_ref=source.at[part, :], dst_ref=held.at[place, part, :], send_sem=side_send.at[depth, piece],
            recv_sem=side_recv.at[depth, piece], device_id={"sp": other}, device_id_type=MESH)

    for piece in range(tiles - 1, -1, -1):
        @pl.when(row < rows - 1)
        def _():
            up_copy(kv_ref, 0, piece).start()

        @pl.when(col == 0)
        def _():
            side_copy(kv_ref, 0, piece).start()

    lane = lax.broadcasted_iota(jnp.int32, (1, width), 1) // HEAD_DIM
    key_row = lax.broadcasted_iota(jnp.int32, (tile, tile), 0)
    key_col = lax.broadcasted_iota(jnp.int32, (tile, tile), 1)
    later = (key_row > key_col).astype(jnp.bfloat16)
    scale = LOG2E / math.sqrt(HEAD_DIM)

    for head in range(heads):
        for query_tile in range(tiles):
            source_rows = slice(query_tile * tile, (query_tile + 1) * tile)
            stacked_rows = slice((query_tile * heads + head) * tile, (query_tile * heads + head + 1) * tile)
            masked[stacked_rows, :] = jnp.where(lane == head, q_ref[source_rows, :], jnp.zeros((), q_ref.dtype))

    def span(source, key_tile, first, last, diagonal):
        stacked_rows = slice(first * heads * tile, last * heads * tile)
        key_rows = slice(key_tile * tile, (key_tile + 1) * tile)
        keys = source[key_rows, :width]
        values = source[key_rows, width:]
        scores = lax.dot_general(masked[stacked_rows, :], keys, (((1,), (1,)), ((), ())), preferred_element_type=jnp.float32) * scale
        soft = lax.log(1.0 + jnp.exp2(-jnp.abs(scores))) * LOG2E
        take = jnp.minimum(scores, 0.0) - soft
        stay = take - scores
        if diagonal:
            query_place = jnp.concatenate([key_row] * ((last - first) * heads), axis=0)
            key_place = jnp.concatenate([key_col] * ((last - first) * heads), axis=0)
            stay = jnp.where(key_place < query_place, stay, 0.0)
        after = jnp.dot(stay.astype(jnp.bfloat16), later, preferred_element_type=jnp.float32)
        before = carry[stacked_rows, :]
        weights = jnp.exp2(take + after + before)
        if diagonal:
            weights = jnp.where(key_place < query_place, weights, 0.0)
        acc[stacked_rows, :] += jnp.dot(weights.astype(jnp.bfloat16), values, preferred_element_type=jnp.float32)
        carry[stacked_rows, :] = before + (after[:, :1] + stay[:, :1])

    acc[...] = jnp.zeros_like(acc)
    carry[...] = jnp.zeros_like(carry)
    for key_tile in range(tiles - 1, -1, -1):
        span(kv_ref, key_tile, key_tile, key_tile + 1, True)
        if key_tile + 1 < tiles:
            span(kv_ref, key_tile, key_tile + 1, tiles, False)

    def receive(depth, piece):
        place = (row - depth) * COLUMNS + col
        up_copy(held.at[place], depth - 1, piece).wait_recv()

        @pl.when(row < rows - 1)
        def _():
            up_copy(held.at[place], depth, piece).start()

        side_copy(held.at[place], depth, piece).start()

    def step(index, unused):
        shard = me - 1 - index
        depth = row - shard // COLUMNS

        @pl.when((index == 0) & (row > 0))
        def _():
            for key_tile in range(tiles - 1, -1, -1):
                receive(1, key_tile)

        source = held.at[shard]
        for key_tile in range(tiles - 1, -1, -1):
            @pl.when(shard % COLUMNS != col)
            def _():
                side_copy(held.at[shard], depth, key_tile).wait_recv()

            @pl.when((shard % COLUMNS == col) & (depth < row))
            def _():
                receive(depth + 1, key_tile)

            span(source, key_tile, 0, tiles, False)
        return unused

    lax.fori_loop(0, me, step, 0)

    def finish(depth, unused):
        @pl.when(row < rows - 1)
        def _():
            for piece in range(tiles):
                up_copy(kv_ref, depth, piece).wait_send()

        @pl.when((col == 0) | (depth > 0))
        def _():
            for piece in range(tiles):
                side_copy(kv_ref, depth, piece).wait_send()

        return unused

    lax.fori_loop(0, row + 1, finish, 0)

    for query_tile in range(tiles):
        mixed = jnp.zeros((tile, width), jnp.float32)
        inverse = jnp.zeros((tile, width), jnp.float32)
        for head in range(heads):
            place = (query_tile * heads + head) * tile
            own = jnp.where(lane == head, acc[place : place + tile, :], 0.0)
            mean = jnp.sum(own * own, axis=1, keepdims=True) * (1.0 / HEAD_DIM)
            mixed = mixed + own
            inverse = jnp.where(lane == head, lax.rsqrt(mean + EPSILON), inverse)
        out_ref[query_tile * tile : (query_tile + 1) * tile, :] = (mixed * inverse * gain_ref[...]).astype(out_ref.dtype)


def round_up(value, unit):
    return (value + unit - 1) // unit * unit


def layer_kernel(
    rows, capacity, span, q_ref, key_ref, value_ref, head_gain_ref, routed_ref, weight_ref, residual_ref, gain_ref, out_weight, shared_gate, shared_up, shared_down, expert_gate,
    expert_up, expert_down, out_ref, kv_ref, heads_ref, meta_ref, held, masked, acc, carry, q_up_send, q_up_recv, q_side_send, q_side_recv, head_rows, meta_all, slots, place, mix, gathered, parts, outgoing, arrived, returned, chained, landed,
    base, gate_sum, up_sum, hidden, w_out, w_sgate, w_sup, w_sdown, w_gate, w_up, w_down, w_sem, head_send, head_recv, meta_send,
    meta_recv, up_send, down_send, block_recv, go_send, go_recv, back_send, back_recv, near_send, near_recv, chain_send, chain_recv,
    far_send, far_recv):
    me = lax.axis_index("sp")
    tp = lax.axis_index("tp")
    row, col = me // COLUMNS, me % COLUMNS
    tp_size = head_rows.shape[0]
    group = COLUMNS * tp_size
    mine = col * tp_size + tp
    _, chunks, _, block_rows, width = outgoing.shape
    local = gate_sum.shape[0]
    count = residual_ref.shape[0]
    picks = routed_ref.shape[0]
    total = group * block_rows
    reach = rows // 2
    half = row // reach
    near_first, far_first = half * reach, (1 - half) * reach
    outward = (1 - half) * (reach - 1 - row) + half * (row - reach)
    inner_row = row + 1 - 2 * half
    bounds = [(e * span // PACK * PACK, round_up((e + 1) * span, PACK)) for e in range(local)]

    loads = []
    for index, (source, target) in enumerate((
            (out_weight, w_out), (shared_gate, w_sgate), (shared_up, w_sup), (shared_down, w_sdown),
            (expert_gate, w_gate), (expert_up, w_up), (expert_down, w_down))):
        loads.append(pltpu.make_async_copy(source, target, w_sem.at[index]))
        loads[-1].start()

    peers = []
    for across in range(COLUMNS - 1, -1, -1):
        for step in list(range(tp_size // 2, tp_size)) + list(range(tp_size // 2)):
            if across or step:
                peers.append(((col + across) % COLUMNS, (tp + step) % tp_size))

    def device(at_row, at_col, at_tp):
        return {"sp": at_row * COLUMNS + at_col, "tp": at_tp}

    def every(ref, semaphore):
        return pltpu.make_async_remote_copy(
            src_ref=ref, dst_ref=ref, send_sem=semaphore, recv_sem=semaphore, device_id=device(row, COLUMNS - 1 - col, tp),
            device_id_type=MESH)

    barrier = pltpu.get_barrier_semaphore()
    for at_col, at_tp in peers:
        pl.semaphore_signal(barrier, inc=1, device_id=device(row, at_col, at_tp), device_id_type=MESH)
    for step in range(1, rows):
        pl.semaphore_signal(barrier, inc=1, device_id=device((row + step) % rows, col, tp), device_id_type=MESH)
    pl.semaphore_wait(barrier, len(peers) + rows - 1)

    kv_ref[:, : key_ref.shape[1]] = key_ref[...]
    kv_ref[:, key_ref.shape[1] :] = value_ref[...]
    meta_ref[:picks, :] = routed_ref[...].astype(jnp.float32)
    meta_ref[picks:, :] = weight_ref[...]
    attention_step(
        rows, q_ref, kv_ref, head_gain_ref, heads_ref, held, masked, acc, carry, q_up_send, q_up_recv, q_side_send, q_side_recv)

    def head_copy(to, source):
        return pltpu.make_async_remote_copy(
            src_ref=heads_ref.at[pl.ds(pl.multiple_of(to * count, count), count), :],
            dst_ref=head_rows.at[source], send_sem=head_send, recv_sem=head_recv,
            device_id=device(row, col, to), device_id_type=MESH)

    def meta_copy(to, source):
        return pltpu.make_async_remote_copy(
            src_ref=meta_ref, dst_ref=meta_all.at[source], send_sem=meta_send, recv_sem=meta_recv,
            device_id=device(to, col, tp), device_id_type=MESH)

    for step in range(1, tp_size):
        head_copy((tp + step) % tp_size, tp).start()
    for step in range(1, rows):
        meta_copy((row + step) % rows, row).start()
    head_rows[tp] = heads_ref[pl.ds(pl.multiple_of(tp * count, count), count), :]
    meta_all[row] = meta_ref[...]

    def up_copy(chunk, block):
        return pltpu.make_async_remote_copy(
            src_ref=gathered.at[chunk, block], dst_ref=gathered.at[chunk, block], send_sem=up_send.at[block],
            recv_sem=block_recv.at[chunk, block], device_id=device(row + 1, col, tp), device_id_type=MESH)

    def down_copy(chunk, block):
        return pltpu.make_async_remote_copy(
            src_ref=gathered.at[chunk, block], dst_ref=gathered.at[chunk, block], send_sem=down_send.at[block],
            recv_sem=block_recv.at[chunk, block], device_id=device(row - 1, col, tp), device_id_type=MESH)

    def from_below(chunk, block):
        up_copy(chunk, block).wait_recv()

        @pl.when(row < rows - 1)
        def _():
            up_copy(chunk, block).start()

    def from_above(chunk, block):
        down_copy(chunk, block).wait_recv()

        @pl.when(row > 0)
        def _():
            down_copy(chunk, block).start()

    def gather_near(chunk):
        for depth in range(1, reach):
            @pl.when(row - depth >= near_first)
            def _():
                from_below(chunk, row - depth)

            @pl.when(row + depth < near_first + reach)
            def _():
                from_above(chunk, row + depth)

    def gather_far(chunk):
        for depth in range(1, rows):
            @pl.when((row - depth >= 0) & (row - depth < near_first))
            def _():
                from_below(chunk, row - depth)

            @pl.when((row + depth >= near_first + reach) & (row + depth < rows))
            def _():
                from_above(chunk, row + depth)

    def go_copy(part, chunk, peer, source):
        at_col, at_tp = peer
        return pltpu.make_async_remote_copy(
            src_ref=outgoing.at[part, chunk, at_col * tp_size + at_tp], dst_ref=arrived.at[part, chunk, source],
            send_sem=go_send.at[part], recv_sem=go_recv.at[part, chunk],
            device_id=device(row, at_col, at_tp), device_id_type=MESH)

    def back_copy(part, chunk, peer, source):
        at_col, at_tp = peer
        return pltpu.make_async_remote_copy(
            src_ref=outgoing.at[part, chunk, at_col * tp_size + at_tp], dst_ref=returned.at[part, chunk, source],
            send_sem=back_send, recv_sem=back_recv.at[part, chunk],
            device_id=device(row, at_col, at_tp), device_id_type=MESH)

    def near_copy(chunk, block, source):
        return pltpu.make_async_remote_copy(
            src_ref=parts.at[chunk, block], dst_ref=landed.at[chunk, source - near_first],
            send_sem=near_send, recv_sem=near_recv.at[chunk],
            device_id=device(block, col, tp), device_id_type=MESH)

    def chain_copy(chunk, index):
        return pltpu.make_async_remote_copy(
            src_ref=parts.at[chunk, far_first + index], dst_ref=chained.at[chunk, index],
            send_sem=chain_send, recv_sem=chain_recv.at[chunk],
            device_id=device(inner_row, col, tp), device_id_type=MESH)

    def far_copy(chunk, index):
        return pltpu.make_async_remote_copy(
            src_ref=parts.at[chunk, far_first + index], dst_ref=landed.at[chunk, reach],
            send_sem=far_send, recv_sem=far_recv.at[chunk],
            device_id=device(far_first + index, col, tp), device_id_type=MESH)

    def dispatch(part, chunk):
        first_block = near_first if part == 0 else far_first
        tokens = gathered[chunk, pl.ds(first_block, reach)].reshape(reach * count, width)
        rows_out = jnp.dot(place[part], tokens, preferred_element_type=jnp.float32).astype(jnp.bfloat16)
        outgoing[part, chunk] = rows_out.reshape(group, block_rows, width)
        arrived[part, chunk, mine] = outgoing[part, chunk, mine]
        for peer in peers:
            go_copy(part, chunk, peer, mine).start()

    def enter(part, chunk):
        every(arrived.at[part, chunk, pl.ds(0, group - 1)], go_recv.at[part, chunk]).wait_recv()
        deep = pl.ds(pl.multiple_of(chunk * width, width), width)
        for expert, (low, high) in enumerate(bounds):
            block = arrived[part, chunk, :, low:high, :].reshape(group * (high - low), width)
            gate_sum[expert] += jnp.dot(block, w_gate[expert, deep, :], preferred_element_type=jnp.float32)
            up_sum[expert] += jnp.dot(block, w_up[expert, deep, :], preferred_element_type=jnp.float32)

    def activate(part):
        for expert in range(local):
            gate = gate_sum[expert]
            hidden[part, expert] = (gate / (1.0 + jnp.exp(-gate)) * up_sum[expert]).astype(jnp.bfloat16)

    def leave(part, chunk):
        wide = pl.ds(pl.multiple_of(chunk * width, width), width)
        downs = [
            jnp.dot(hidden[part, expert], w_down[expert, :, wide], preferred_element_type=jnp.float32).reshape(group, high - low, width)
            for expert, (low, high) in enumerate(bounds)]
        inside = lax.broadcasted_iota(jnp.int32, (1, PACK, 1), 1)
        for tile in range(0, block_rows, PACK):
            value = None
            for expert, (low, high) in enumerate(bounds):
                if low <= tile < high:
                    piece = downs[expert][:, tile - low : tile - low + PACK, :]
                    value = piece if value is None else jnp.where(inside + tile >= expert * span, piece, value)
            outgoing[part, chunk, :, tile : tile + PACK, :] = value.astype(jnp.bfloat16)
        returned[part, chunk, mine] = outgoing[part, chunk, mine]
        for peer in peers:
            back_copy(part, chunk, peer, mine).start()

    def combine(part, chunk):
        every(returned.at[part, chunk, pl.ds(0, group - 1)], back_recv.at[part, chunk]).wait_recv()
        return returned[part, chunk].reshape(total, width)

    def combine_near(chunk):
        results = combine(0, chunk)
        for step in range(1, reach):
            block = near_first + (row - near_first + step) % reach
            parts[chunk, block] = jnp.dot(mix[block], results, preferred_element_type=jnp.float32).astype(jnp.bfloat16)
        base[chunk] += jnp.dot(mix[row], results, preferred_element_type=jnp.float32)
        for step in range(1, reach):
            near_copy(chunk, near_first + (row - near_first + step) % reach, row).start()

    def combine_far(chunk):
        results = combine(1, chunk)
        for index in range(reach):
            block = far_first + index
            parts[chunk, block] = jnp.dot(mix[block], results, preferred_element_type=jnp.float32).astype(jnp.bfloat16)

        @pl.when(outward == reach - 1)
        def _():
            onward(chunk)

    def onward(chunk):
        for index in range(reach):
            @pl.when(outward > 0)
            def _():
                chain_copy(chunk, index).start()

            @pl.when(outward == 0)
            def _():
                far_copy(chunk, index).start()

    def fold(chunk):
        @pl.when(outward < reach - 1)
        def _():
            every(chained.at[chunk], chain_recv.at[chunk]).wait_recv()
            for index in range(reach):
                block = far_first + index
                parts[chunk, block] = (
                    parts[chunk, block].astype(jnp.float32) + chained[chunk, index].astype(jnp.float32)).astype(jnp.bfloat16)
            onward(chunk)

    def loop(first, last, step):
        def one(index, unused):
            step(index)
            return unused

        lax.fori_loop(first, last, one, 0)

    loads[0].wait()
    every(head_rows.at[pl.ds(0, tp_size - 1)], head_recv).wait_recv()
    token_heads = jnp.concatenate([head_rows[source] for source in range(tp_size)], axis=1)
    branch = jnp.dot(token_heads, w_out[...], preferred_element_type=jnp.float32)
    stream = (residual_ref[...].astype(jnp.float32) + branch).astype(jnp.bfloat16).astype(jnp.float32)
    inverse = lax.rsqrt(jnp.mean(stream * stream, axis=1, keepdims=True) + EPSILON)
    normed = (stream * inverse * gain_ref[...]).astype(jnp.bfloat16)
    for chunk in range(chunks):
        columns = slice(chunk * width, (chunk + 1) * width)
        base[chunk] = stream[:, columns]
        gathered[chunk, row] = normed[:, columns]

    def send_own(chunk):
        @pl.when(row < rows - 1)
        def _():
            up_copy(chunk, row).start()

        @pl.when(row > 0)
        def _():
            down_copy(chunk, row).start()

    loop(0, chunks, send_own)
    every(meta_all.at[pl.ds(0, rows - 1)], meta_recv).wait_recv()
    expert_place = lax.broadcasted_iota(jnp.int32, (group * local, count), 0).astype(jnp.float32)
    slot_place = lax.broadcasted_iota(jnp.int32, (total, count), 0).astype(jnp.float32)
    before = lax.broadcasted_iota(jnp.int32, (count, count), 0)
    after = lax.broadcasted_iota(jnp.int32, (count, count), 1)
    earlier = (before < after).astype(jnp.bfloat16)
    lowest = (row * (group * local)).astype(jnp.float32)
    for part in range(2):
        for index in range(reach):
            block = (near_first if part == 0 else far_first) + index
            meta = meta_all[block]
            chosen = [meta[k : k + 1, :] - lowest for k in range(picks)]
            tables = [jnp.where(expert_place == chosen[k], 1.0, 0.0) for k in range(picks)]
            tally = jnp.dot(sum(tables).astype(jnp.bfloat16), earlier, preferred_element_type=jnp.float32)
            placed = jnp.zeros((total, count), jnp.float32)
            for k in range(picks):
                ranking = jnp.sum(tables[k] * tally, axis=0, keepdims=True)
                inside = (chosen[k] >= 0.0) & (chosen[k] < float(group * local))
                owner = jnp.floor(chosen[k] * (1.0 / local))
                start = owner * float(block_rows) + (chosen[k] - owner * float(local)) * float(span)
                slot = jnp.where(inside, start + (index * capacity + ranking), -1.0)
                slots[block, k : k + 1, :] = slot
                placed = jnp.where(slot_place == slot, 1.0, placed)
            place[part, :, index * count : (index + 1) * count] = placed.astype(jnp.bfloat16)

    for block in range(rows):
        weighed = jnp.zeros((total, count), jnp.float32)
        for k in range(picks):
            slot = slots[block, k : k + 1, :]
            weighed = jnp.where(slot_place == slot, meta_all[block, picks + k : picks + k + 1, :], weighed)
        mix[block] = weighed.T.astype(jnp.bfloat16)

    gate_sum[...] = jnp.zeros_like(gate_sum)
    up_sum[...] = jnp.zeros_like(up_sum)
    for load in loads[1:4]:
        load.wait()
    shared = jnp.dot(normed, w_sgate[...], preferred_element_type=jnp.float32)
    shared = shared / (1.0 + jnp.exp(-shared)) * jnp.dot(normed, w_sup[...], preferred_element_type=jnp.float32)
    shared = shared.astype(jnp.bfloat16)
    for chunk in range(chunks):
        columns = slice(chunk * width, (chunk + 1) * width)
        base[chunk] += jnp.dot(shared, w_sdown[:, columns], preferred_element_type=jnp.float32)

    def near_step(chunk):
        gather_near(chunk)
        dispatch(0, chunk)

    loop(0, chunks, near_step)
    for load in loads[4:]:
        load.wait()

    split = chunks // 2

    def far_step(chunk):
        gather_far(chunk)
        dispatch(1, chunk)

        @pl.when(chunk < split)
        def _():
            enter(0, 2 * chunk)
            enter(0, 2 * chunk + 1)

        @pl.when(chunk == split)
        def _():
            activate(0)
            gate_sum[...] = jnp.zeros_like(gate_sum)
            up_sum[...] = jnp.zeros_like(up_sum)

        @pl.when(chunk >= split)
        def _():
            enter(1, chunk - split)

    loop(0, chunks, far_step)
    every(outgoing.at[0, :, pl.ds(0, group - 1)], go_send.at[0]).wait_send()
    loop(0, FIRST, lambda chunk: leave(0, chunk))
    loop(chunks - split, chunks, lambda chunk: enter(1, chunk))
    activate(1)
    every(outgoing.at[1, :, pl.ds(0, group - 1)], go_send.at[1]).wait_send()

    loop(0, AHEAD, lambda chunk: leave(1, chunk))

    def far_back(index):
        @pl.when(index + AHEAD < chunks)
        def _():
            leave(1, index + AHEAD)

        @pl.when(index + AHEAD >= chunks)
        def _():
            leave(0, index + AHEAD - chunks + FIRST)

        @pl.when(index < FIRST)
        def _():
            combine_near(index)

        combine_far(index)

        @pl.when(index >= LAG)
        def _():
            fold(index - LAG)

    loop(0, chunks, far_back)

    def close(chunk):
        value = base[chunk]
        far_copy(chunk, 0).wait_recv()
        value += landed[chunk, reach].astype(jnp.float32)
        every(landed.at[chunk, pl.ds(0, reach - 1)], near_recv.at[chunk]).wait_recv()
        for step in range(1, reach):
            source = near_first + (row - near_first + step) % reach
            value += landed[chunk, source - near_first].astype(jnp.float32)
        out_ref[:, pl.ds(pl.multiple_of(chunk * width, width), width)] = value.astype(out_ref.dtype)

    def near_back(index):
        @pl.when(index + AHEAD < chunks)
        def _():
            leave(0, index + AHEAD)

        combine_near(index)
        turn = index - FIRST

        @pl.when((turn >= 1) & (turn <= LAG))
        def _():
            fold(chunks - LAG + turn - 1)

        @pl.when(turn >= LAG)
        def _():
            close(turn - LAG)

    loop(FIRST, chunks, near_back)
    loop(chunks - FIRST - LAG, chunks, close)
    every(outgoing.at[:, :, pl.ds(0, group - 1)], back_send).wait_send()
    every(parts.at[:, pl.ds(0, reach - 1)], near_send).wait_send()

    @pl.when(outward > 0)
    def _():
        every(parts.at[:, pl.ds(0, reach)], chain_send).wait_send()

    @pl.when(outward == 0)
    def _():
        every(parts.at[:, pl.ds(0, reach)], far_send).wait_send()

    @pl.when(row < rows - 1)
    def _():
        loop(0, row + 1, lambda block: every(gathered.at[:, block], up_send.at[block]).wait_send())

    @pl.when(row > 0)
    def _():
        loop(row, rows, lambda block: every(gathered.at[:, block], down_send.at[block]).wait_send())

    every(head_rows.at[pl.ds(0, tp_size - 1)], head_send).wait_send()
    every(meta_all.at[pl.ds(0, rows - 1)], meta_send).wait_send()


def layer(
    queries, key_heads, value_heads, head_gain, residual, out_weight, norm_gain, shared_gate, shared_up, shared_down, expert_gate, expert_up, expert_down,
    routed_experts, route_weights):
    count, picks = routed_experts.shape
    model = residual.shape[1]
    sp_size, tp_size = lax.axis_size("sp"), lax.axis_size("tp")
    rows, group = sp_size // COLUMNS, COLUMNS * tp_size
    reach = rows // 2
    local, _, inner = expert_gate.shape
    expert_count = local * sp_size * tp_size
    capacity = max(2, 3 * count * picks // (2 * expert_count))
    span = round_up(reach * capacity, 8)
    block_rows = round_up(local * span, PACK)
    total = group * block_rows
    wide = max(round_up((e + 1) * span, PACK) - e * span // PACK * PACK for e in range(local))
    width = model // CHUNKS
    seq, head_width = queries.shape
    heads = head_width // HEAD_DIM
    pieces = -(-seq // TILE)
    vmem = pl.BlockSpec(memory_space=pltpu.VMEM)
    hbm = pl.BlockSpec(memory_space=pl.ANY)
    half = jnp.bfloat16

    return pl.pallas_call(
        functools.partial(layer_kernel, rows, capacity, span),
        out_shape=jax.ShapeDtypeStruct((count, model), half),
        in_specs=[vmem] * 8 + [hbm] * 7,
        out_specs=vmem,
        scratch_shapes=[
            pltpu.VMEM((seq, 2 * head_width), half),
            pltpu.VMEM((seq, head_width), half),
            pltpu.VMEM((2 * picks, count), jnp.float32),
            pltpu.VMEM((sp_size, seq, 2 * head_width), half),
            pltpu.VMEM((heads * seq, head_width), half),
            pltpu.VMEM((heads * seq, head_width), jnp.float32),
            pltpu.VMEM((heads * seq, 1), jnp.float32),
            *[pltpu.SemaphoreType.DMA((rows, pieces))] * 4,
            pltpu.VMEM((tp_size, count, head_width), half),
            pltpu.VMEM((rows, 2 * picks, count), jnp.float32),
            pltpu.VMEM((rows, 2 * picks, count), jnp.float32),
            pltpu.VMEM((2, total, reach * count), half),
            pltpu.VMEM((rows, count, total), half),
            pltpu.VMEM((CHUNKS, rows, count, width), half),
            pltpu.VMEM((CHUNKS, rows, count, width), half),
            pltpu.VMEM((2, CHUNKS, group, block_rows, width), half),
            pltpu.VMEM((2, CHUNKS, group, block_rows, width), half),
            pltpu.VMEM((2, CHUNKS, group, block_rows, width), half),
            pltpu.VMEM((CHUNKS, reach, count, width), half),
            pltpu.VMEM((CHUNKS, reach + 1, count, width), half),
            pltpu.VMEM((CHUNKS, count, width), jnp.float32),
            pltpu.VMEM((local, group * wide, inner), jnp.float32),
            pltpu.VMEM((local, group * wide, inner), jnp.float32),
            pltpu.VMEM((2, local, group * wide, inner), half),
            pltpu.VMEM(out_weight.shape, half),
            pltpu.VMEM(shared_gate.shape, half),
            pltpu.VMEM(shared_up.shape, half),
            pltpu.VMEM(shared_down.shape, half),
            pltpu.VMEM(expert_gate.shape, half),
            pltpu.VMEM(expert_up.shape, half),
            pltpu.VMEM(expert_down.shape, half),
            pltpu.SemaphoreType.DMA((7,)),
            *[pltpu.SemaphoreType.DMA] * 4,
            *[pltpu.SemaphoreType.DMA((rows,))] * 2,
            pltpu.SemaphoreType.DMA((CHUNKS, rows)),
            pltpu.SemaphoreType.DMA((2,)),
            pltpu.SemaphoreType.DMA((2, CHUNKS)),
            pltpu.SemaphoreType.DMA,
            pltpu.SemaphoreType.DMA((2, CHUNKS)),
            *[pltpu.SemaphoreType.DMA, pltpu.SemaphoreType.DMA((CHUNKS,))] * 3,
        ],
        compiler_params=pltpu.CompilerParams(collective_id=0, has_side_effects=True, vmem_limit_bytes=VMEM_LIMIT),
        name="layer",
    )(queries, key_heads, value_heads, head_gain.reshape(1, head_width), routed_experts.T, route_weights.T, residual, norm_gain.reshape(1, model), out_weight, shared_gate, shared_up, shared_down,
      expert_gate, expert_up, expert_down)


def body(
    queries,
    key_heads,
    value_heads,
    head_gain,
    residual,
    out_weight,
    norm_gain,
    shared_gate,
    shared_up,
    shared_down,
    expert_gate,
    expert_up,
    expert_down,
    routed_experts,
    route_weights,
):
    return layer(
        queries, key_heads, value_heads, head_gain, residual, out_weight, norm_gain, shared_gate, shared_up, shared_down,
        expert_gate, expert_up, expert_down, routed_experts, route_weights)


def solution(mesh):
    return jax.shard_map(
        body,
        mesh=mesh,
        in_specs=(
            P("sp", "tp"),
            P("sp", "tp"),
            P("sp", "tp"),
            P("tp"),
            P(("sp", "tp"), None),
            P(),
            P(),
            P(),
            P(),
            P(),
            P(("sp", "tp"), None, None),
            P(("sp", "tp"), None, None),
            P(("sp", "tp"), None, None),
            P(("sp", "tp"), None),
            P(("sp", "tp"), None),
        ),
        out_specs=P(("sp", "tp"), None),
        check_vma=False,
    )
```

time: 145 us -> 123 us (0.85)
  Pallas kernels: 139 us -> 121 us
  other arithmetic: 3.64 us -> 0 us
    pallas_call x2 -> x1, Pallas kernels: 139 us -> 121 us  [layer(): pl.pallas_call(functools.partial(layer_kernel, rows, capacity, span), out...]
    concatenate x2 -> x0, other arithmetic: 2.96 us -> none  [the longest x1 1.7 us: attention(): both = jnp.concatenate([key_heads, value_heads], axis=1)]
where the time goes in v3:
time: 123 us
  Pallas kernels  121 us (98%)
  local copies, waits for them, and re-layouts  1.88 us (2%)
    pallas_call x1, Pallas kernels, layer(): pl.pallas_call(functools.partial(layer_kernel, rows, capacity, span), out...  121 us

profile of v3, /device:TPU:0, one launch (start us, length us, event | category | flops | bytes accessed | tf_op | source)
XLA Modules:
  0.0 122.7 jit_solution(15848450033153206413)
XLA Ops:
  0.0 120.8 %layer.1 = bf16[128,2048]{1,0:T(8,128)(2,1)} custom-call(bf16[512,128]{1,0:T(8,128)(2,1)} %q_ref.1, bf16[512,128]{1,0:T(8,128)(2,1)} %key_ref.1, bf16[512,128]{1,0:T(8,128)(2,1)} %value_ref.1, f32[1,128]{1,0:T(1,128)} %bitcast.7, s32[4,128]{1,0:T(4,128)} %bitcast.5, f32[4,128]{1,0:T(4,128)} %bitcast.6, bf16[128,2048]{1,0:T(8,128)(2,1)} %residual_ref.1, ...), custom_call_target="tpu_custom_call" | custom-call | tf_op jit(solution)/shard_map/layer/pallas_call | solution.py:605
  120.8 1.9 %copy.17 = bf16[128,2048]{1,0:T(8,128)(2,1)} copy(bf16[128,2048]{1,0:T(8,128)(2,1)} %layer.1) | data formatting | bytes 1048576

commit v4 on v3

--- a/solution.py
+++ b/solution.py
@@ -21,6 +21,7 @@
 FIRST = 2
 LAG = 3
 AHEAD = 3
+SPLIT = 2
 PACK = 16
 VMEM_LIMIT = 67043328
 
@@ -34,21 +35,27 @@
     tiles = seq // tile
     other = row * COLUMNS + (COLUMNS - 1 - col)
 
+    short = tile // SPLIT
+
     def up_copy(source, depth, piece):
         place = (row - depth) * COLUMNS + col
-        part = pl.ds(piece * tile, tile)
-        return pltpu.make_async_remote_copy(
-            src_ref=source.at[part, :], dst_ref=held.at[place, part, :], send_sem=up_send.at[depth, piece],
+        part = pl.ds(piece * short, short)
+        return pltpu.make_async_remote_copy(
+            src_ref=source.at[part, :], dst_ref=held.at[place, part, :], send_sem=up_send.at[depth],
             recv_sem=up_recv.at[depth, piece], device_id={"sp": me + COLUMNS}, device_id_type=MESH)
 
     def side_copy(source, depth, piece):
         place = (row - depth) * COLUMNS + col
-        part = pl.ds(piece * tile, tile)
-        return pltpu.make_async_remote_copy(
-            src_ref=source.at[part, :], dst_ref=held.at[place, part, :], send_sem=side_send.at[depth, piece],
+        part = pl.ds(piece * short, short)
+        return pltpu.make_async_remote_copy(
+            src_ref=source.at[part, :], dst_ref=held.at[place, part, :], send_sem=side_send.at[depth],
             recv_sem=side_recv.at[depth, piece], device_id={"sp": other}, device_id_type=MESH)
 
-    for piece in range(tiles - 1, -1, -1):
+    def whole_copy(semaphore):
+        return pltpu.make_async_remote_copy(
+            src_ref=kv_ref, dst_ref=kv_ref, send_sem=semaphore, recv_sem=semaphore, device_id={"sp": other}, device_id_type=MESH)
+
+    for piece in range(tiles * SPLIT - 1, -1, -1):
         @pl.when(row < rows - 1)
         def _():
             up_copy(kv_ref, 0, piece).start()
@@ -97,15 +104,16 @@
         if key_tile + 1 < tiles:
             span(kv_ref, key_tile, key_tile + 1, tiles, False)
 
-    def receive(depth, piece):
+    def receive(depth, key_tile):
         place = (row - depth) * COLUMNS + col
-        up_copy(held.at[place], depth - 1, piece).wait_recv()
-
-        @pl.when(row < rows - 1)
-        def _():
-            up_copy(held.at[place], depth, piece).start()
-
-        side_copy(held.at[place], depth, piece).start()
+        for piece in range((key_tile + 1) * SPLIT - 1, key_tile * SPLIT - 1, -1):
+            up_copy(held.at[place], depth - 1, piece).wait_recv()
+
+            @pl.when(row < rows - 1)
+            def _():
+                up_copy(held.at[place], depth, piece).start()
+
+            side_copy(held.at[place], depth, piece).start()
 
     def step(index, unused):
         shard = me - 1 - index
@@ -120,7 +128,8 @@
         for key_tile in range(tiles - 1, -1, -1):
             @pl.when(shard % COLUMNS != col)
             def _():
-                side_copy(held.at[shard], depth, key_tile).wait_recv()
+                for piece in range((key_tile + 1) * SPLIT - 1, key_tile * SPLIT - 1, -1):
+                    side_copy(held.at[shard], depth, piece).wait_recv()
 
             @pl.when((shard % COLUMNS == col) & (depth < row))
             def _():
@@ -134,13 +143,11 @@
     def finish(depth, unused):
         @pl.when(row < rows - 1)
         def _():
-            for piece in range(tiles):
-                up_copy(kv_ref, depth, piece).wait_send()
+            whole_copy(up_send.at[depth]).wait_send()
 
         @pl.when((col == 0) | (depth > 0))
         def _():
-            for piece in range(tiles):
-                side_copy(kv_ref, depth, piece).wait_send()
+            whole_copy(side_send.at[depth]).wait_send()
 
         return unused
 
@@ -184,6 +191,7 @@
     near_first, far_first = half * reach, (1 - half) * reach
     outward = (1 - half) * (reach - 1 - row) + half * (row - reach)
     inner_row = row + 1 - 2 * half
+    relays = half * ((2 * reach - 2 - outward) // reach)
     bounds = [(e * span // PACK * PACK, round_up((e + 1) * span, PACK)) for e in range(local)]
 
     loads = []
@@ -218,6 +226,15 @@
     kv_ref[:, key_ref.shape[1] :] = value_ref[...]
     meta_ref[:picks, :] = routed_ref[...].astype(jnp.float32)
     meta_ref[picks:, :] = weight_ref[...]
+    meta_all[row] = meta_ref[...]
+
+    def meta_copy(to, source):
+        return pltpu.make_async_remote_copy(
+            src_ref=meta_ref, dst_ref=meta_all.at[source], send_sem=meta_send, recv_sem=meta_recv,
+            device_id=device(to, col, tp), device_id_type=MESH)
+
+    for step in range(1, rows):
+        meta_copy((row + step) % rows, row).start()
     attention_step(
         rows, q_ref, kv_ref, head_gain_ref, heads_ref, held, masked, acc, carry, q_up_send, q_up_recv, q_side_send, q_side_recv)
 
@@ -227,17 +244,9 @@
             dst_ref=head_rows.at[source], send_sem=head_send, recv_sem=head_recv,
             device_id=device(row, col, to), device_id_type=MESH)
 
-    def meta_copy(to, source):
-        return pltpu.make_async_remote_copy(
-            src_ref=meta_ref, dst_ref=meta_all.at[source], send_sem=meta_send, recv_sem=meta_recv,
-            device_id=device(to, col, tp), device_id_type=MESH)
-
     for step in range(1, tp_size):
         head_copy((tp + step) % tp_size, tp).start()
-    for step in range(1, rows):
-        meta_copy((row + step) % rows, row).start()
     head_rows[tp] = heads_ref[pl.ds(pl.multiple_of(tp * count, count), count), :]
-    meta_all[row] = meta_ref[...]
 
     def up_copy(chunk, block):
         return pltpu.make_async_remote_copy(
@@ -473,6 +482,10 @@
         gather_near(chunk)
         dispatch(0, chunk)
 
+        @pl.when(relays == 1)
+        def _():
+            gather_far(chunk)
+
     loop(0, chunks, near_step)
     for load in loads[4:]:
         load.wait()
@@ -480,7 +493,10 @@
     split = chunks // 2
 
     def far_step(chunk):
-        gather_far(chunk)
+        @pl.when(relays == 0)
+        def _():
+            gather_far(chunk)
+
         dispatch(1, chunk)
 
         @pl.when(chunk < split)
@@ -516,16 +532,13 @@
         def _():
             leave(0, index + AHEAD - chunks + FIRST)
 
-        @pl.when(index < FIRST)
-        def _():
-            combine_near(index)
-
         combine_far(index)
 
         @pl.when(index >= LAG)
         def _():
             fold(index - LAG)
 
+    loop(0, FIRST, combine_near)
     loop(0, chunks, far_back)
 
     def close(chunk):
@@ -597,7 +610,7 @@
     width = model // CHUNKS
     seq, head_width = queries.shape
     heads = head_width // HEAD_DIM
-    pieces = -(-seq // TILE)
+    pieces = max(seq // TILE, 1) * SPLIT
     vmem = pl.BlockSpec(memory_space=pltpu.VMEM)
     hbm = pl.BlockSpec(memory_space=pl.ANY)
     half = jnp.bfloat16
@@ -615,7 +628,7 @@
             pltpu.VMEM((heads * seq, head_width), half),
             pltpu.VMEM((heads * seq, head_width), jnp.float32),
             pltpu.VMEM((heads * seq, 1), jnp.float32),
-            *[pltpu.SemaphoreType.DMA((rows, pieces))] * 4,
+            *[pltpu.SemaphoreType.DMA((rows,)), pltpu.SemaphoreType.DMA((rows, pieces))] * 2,
             pltpu.VMEM((tp_size, count, head_width), half),
             pltpu.VMEM((rows, 2 * picks, count), jnp.float32),
             pltpu.VMEM((rows, 2 * picks, count), jnp.float32),

time: 123 us -> 119 us (0.967)
  Pallas kernels: 121 us -> 117 us
    pallas_call x1, Pallas kernels: 121 us -> 117 us  [layer(): pl.pallas_call(functools.partial(layer_kernel, rows, capacity, span), out...]
where the time goes in v4:
time: 119 us
  Pallas kernels  117 us (98%)
  local copies, waits for them, and re-layouts  1.88 us (2%)
    pallas_call x1, Pallas kernels, layer(): pl.pallas_call(functools.partial(layer_kernel, rows, capacity, span), out...  117 us

profile of v4, /device:TPU:0, one launch (start us, length us, event | category | flops | bytes accessed | tf_op | source)
XLA Modules:
  0.0 118.6 jit_solution(8430131469888250192)
XLA Ops:
  0.0 116.7 %layer.1 = bf16[128,2048]{1,0:T(8,128)(2,1)} custom-call(bf16[512,128]{1,0:T(8,128)(2,1)} %q_ref.1, bf16[512,128]{1,0:T(8,128)(2,1)} %key_ref.1, bf16[512,128]{1,0:T(8,128)(2,1)} %value_ref.1, f32[1,128]{1,0:T(1,128)} %bitcast.7, s32[4,128]{1,0:T(4,128)} %bitcast.5, f32[4,128]{1,0:T(4,128)} %bitcast.6, bf16[128,2048]{1,0:T(8,128)(2,1)} %residual_ref.1, ...), custom_call_target="tpu_custom_call" | custom-call | tf_op jit(solution)/shard_map/layer/pallas_call | solution.py:618
  116.7 1.9 %copy.17 = bf16[128,2048]{1,0:T(8,128)(2,1)} copy(bf16[128,2048]{1,0:T(8,128)(2,1)} %layer.1) | data formatting | bytes 1048576
